TPU v7x, 128 devices: a whole 4x4x4 slice. The times are simulated.
128 devices in a mesh: ep: 32 (over z, y, core), tp: 4 (over x).
Axes of the slice: x: 4, y: 4, z: 4, core: 2. Of those that a mesh axis runs over, the one named last changes fastest.
Arguments:
- query_rows: bfloat16 [65536, 1024], P('ep', 'tp'), may hold values from -6 to 6
- key_rows: bfloat16 [65536, 1024], P('ep', 'tp'), may hold values from -6 to 6
- value_rows: bfloat16 [65536, 2048], P('ep', 'tp'), may hold values from -6 to 6
- gate_rows: bfloat16 [65536, 2048], P('ep', 'tp'), may hold values from -6 to 6
- log_decay: float32 [8, 65536], P('tp', 'ep'), may hold values from -1 to 0
- out_proj: bfloat16 [2048, 2048], P('tp'), may hold values from -0.125 to 0.125
- moe_input: bfloat16 [16384, 2048], P(('ep', 'tp')), may hold values from -6 to 6
- norm_gain: float32 [2048], replicated, may hold values from 0.1 to 1.9
- routing: int32 [16384, 4], P(('ep', 'tp')), may hold values from 0 to 127, all different within a row; in each aligned block of 128 rows (0 to 127, 128 to 255, ...) at most 8 rows name the same one
- route_weight: float32 [16384, 4], P(('ep', 'tp')), may hold values from 0.2 to 1
- expert_gate: bfloat16 [128, 2048, 512], P(('ep', 'tp')), may hold values from -0.125 to 0.125
- expert_up: bfloat16 [128, 2048, 512], P(('ep', 'tp')), may hold values from -0.125 to 0.125
- expert_down: bfloat16 [128, 512, 2048], P(('ep', 'tp')), may hold values from -0.25 to 0.25
- shared_gate: bfloat16 [2048, 512], replicated, may hold values from -0.125 to 0.125
- shared_up: bfloat16 [2048, 512], replicated, may hold values from -0.125 to 0.125
- shared_down: bfloat16 [512, 2048], replicated, may hold values from -0.25 to 0.25
Outputs:
- mixer_out: bfloat16 [65536, 2048], P(('ep', 'tp'))
- moe_out: bfloat16 [16384, 2048], P(('ep', 'tp'))
Inputs may be any that keep to these rules, and one draw needn't show every extreme that they name: `routing`: within the rows of one device no expert is named more than 8 times.
All inputs are finite; a program needn't handle non-finite values.
Results may differ from a plain program's by a relative error of at most 0.019.
Values may be sent and summed in bfloat16 or wider, within the bound.
A program may use at most 128 MiB of HBM per device.

v0:
```python
import jax
import jax.numpy as jnp
from jax import lax
from jax.sharding import Mesh
from jax.sharding import PartitionSpec as P

DK = 128
DV = 256
BLOCK = 128
EP = ("ep_0", "ep_1", "ep_2")
EP_TP = ("ep_0", "ep_1", "ep_2", "tp")


EPS = 1e-06


def neutral_like(x, identity):
    return jax.tree.map(
        lambda part, zero: jnp.zeros_like(part) + jnp.asarray(zero, part.dtype), x, identity
    )


def carried_in(x, axes, combine, identity):
    before = start = neutral_like(x, identity)
    subtotal = x
    for axis in reversed(axes):
        peers, place = (lax.axis_size(axis), lax.axis_index(axis))
        pieces = jax.tree.map(
            lambda part, kind: lax.all_gather(part.astype(kind), axis),
            subtotal,
            (jnp.bfloat16, jnp.bfloat16),
        )
        inside, subtotal = (start, start)
        for k in range(peers):
            passed = k < place
            subtotal = combine(
                subtotal, jax.tree.map(lambda part, own: part[k].astype(own.dtype), pieces, x)
            )
            inside = jax.tree.map(lambda new, old: jnp.where(passed, new, old), subtotal, inside)
        before = combine(inside, before)
    return before


def join_states(earlier, later):
    return (earlier[0] * later[0], later[0][:, None, None] * earlier[1] + later[1])


def mixer_half(query_rows, key_rows, value_rows, gate_rows, log_decay, out_proj):
    n_rows = query_rows.shape[0]
    n_heads = query_rows.shape[1] // DK
    n_blocks = n_rows // BLOCK
    score_scale = DK ** (-0.5)
    q_blocks = query_rows.reshape(n_blocks, BLOCK, n_heads, DK)
    k_blocks = key_rows.reshape(n_blocks, BLOCK, n_heads, DK)
    v_blocks = value_rows.reshape(n_blocks, BLOCK, n_heads, DV)
    cum_decay = jnp.cumsum(log_decay.reshape(n_heads, n_blocks, BLOCK), axis=2)
    block_count = cum_decay[:, :, -1]
    causal = jnp.arange(BLOCK)[:, None] >= jnp.arange(BLOCK)[None, :]
    log_gap = jnp.where(causal, cum_decay[:, :, :, None] - cum_decay[:, :, None, :], 0.0)
    decay_mat = jnp.where(causal, jnp.exp(log_gap), 0.0)
    retention_scores = jnp.einsum(
        "bnhd,bmhd->hbnm", q_blocks, k_blocks, preferred_element_type=jnp.float32
    )
    weight = (retention_scores * score_scale * decay_mat).astype(jnp.bfloat16)
    inner_out = jnp.einsum("hbnm,bmhe->bnhe", weight, v_blocks, preferred_element_type=jnp.float32)
    key_scale = (score_scale * jnp.exp(block_count[:, :, None] - cum_decay)).transpose(1, 2, 0)
    decayed_key_rows = (k_blocks.astype(jnp.float32) * key_scale[..., None]).astype(jnp.bfloat16)
    update = jnp.einsum(
        "bmhd,bmhe->bhde", decayed_key_rows, v_blocks, preferred_element_type=jnp.float32
    )

    def advance(carried_state, block_in):
        shrink_by, added = block_in
        return (carried_state * shrink_by[:, None, None] + added, carried_state)

    local_end, local_prev = lax.scan(
        advance, jnp.zeros((n_heads, DK, DV), jnp.float32), (jnp.exp(block_count).T, update)
    )
    device_shrink = jnp.exp(jnp.sum(block_count, axis=1))
    prefix = carried_in(
        (device_shrink, local_end),
        EP,
        join_states,
        (jnp.ones_like(device_shrink), jnp.zeros_like(local_end)),
    )
    incoming = prefix[1]
    block_start = jnp.cumsum(block_count, axis=1) - block_count
    state_prev = local_prev + jnp.exp(block_start).T[:, :, None, None] * incoming[None]
    cross_out = jnp.einsum(
        "bnhd,bhde->bnhe",
        q_blocks,
        state_prev.astype(jnp.bfloat16),
        preferred_element_type=jnp.float32,
    )
    cross_out = cross_out * jnp.exp(cum_decay).transpose(1, 2, 0)[..., None]
    raw_out = (inner_out + cross_out).reshape(n_rows, n_heads, DV)
    avg_out = jnp.mean(raw_out, axis=-1, keepdims=True)
    spread = jnp.mean(jnp.square(raw_out - avg_out), axis=-1, keepdims=True)
    normed = (raw_out - avg_out) * lax.rsqrt(spread + EPS)
    gate_act = jax.nn.silu(gate_rows.astype(jnp.float32).reshape(n_rows, n_heads, DV))
    retained = (gate_act * normed).reshape(n_rows, n_heads * DV).astype(jnp.bfloat16)
    return lax.psum_scatter(
        jnp.dot(retained, out_proj, preferred_element_type=jnp.float32).astype(jnp.bfloat16),
        "tp",
        scatter_dimension=0,
        tiled=True,
    )


def expert_apply(inputs, w_gate, w_up, w_down):
    gate_act = jnp.dot(inputs, w_gate, preferred_element_type=jnp.float32)
    up_act = jnp.dot(inputs, w_up, preferred_element_type=jnp.float32)
    hidden = (jax.nn.silu(gate_act) * up_act).astype(jnp.bfloat16)
    return jnp.dot(hidden, w_down, preferred_element_type=jnp.float32)


def moe_half(
    moe_input,
    norm_gain,
    routing,
    route_weight,
    expert_gate,
    expert_up,
    expert_down,
    shared_gate,
    shared_up,
    shared_down,
):
    as_float = moe_input.astype(jnp.float32)
    moe_normed = (
        as_float
        * lax.rsqrt(jnp.mean(as_float * as_float, axis=-1, keepdims=True) + EPS)
        * norm_gain
    ).astype(jnp.bfloat16)
    n_tokens = routing.shape[0]
    n_visits = routing.shape[1]
    model_width = moe_normed.shape[1]
    experts = lax.axis_size(EP) * lax.axis_size("tp")
    capacity = 2 * n_tokens * n_visits // experts
    flat_route = routing.reshape(-1)
    onehot = (flat_route[:, None] == jnp.arange(experts, dtype=jnp.int32)[None, :]).astype(
        jnp.int32
    )
    slot_rank = jnp.sum(jnp.cumsum(onehot, axis=0) * onehot, axis=1) - 1
    slot_index = flat_route * capacity + slot_rank
    source = jnp.arange(n_tokens * n_visits, dtype=jnp.int32) // n_visits
    outgoing = (
        jnp.zeros((experts * capacity, model_width), jnp.bfloat16)
        .at[slot_index]
        .set(moe_normed[source])
    )
    w_gate = expert_gate[0]
    w_up = expert_up[0]
    w_down = expert_down[0]
    received = lax.all_to_all(
        outgoing.reshape(experts, capacity, model_width),
        EP_TP,
        split_axis=0,
        concat_axis=0,
        tiled=True,
    )
    served = (
        expert_apply(received.reshape(-1, model_width), w_gate, w_up, w_down)
        .astype(jnp.bfloat16)
        .reshape(received.shape)
    )
    returned = lax.all_to_all(served, EP_TP, split_axis=0, concat_axis=0, tiled=True)
    picked = returned.reshape(experts * capacity, model_width)[slot_index].astype(jnp.float32)
    weighted = picked * route_weight.reshape(-1)[:, None]
    routed = jnp.sum(weighted.reshape(n_tokens, n_visits, model_width), axis=1)
    shared = expert_apply(moe_normed, shared_gate, shared_up, shared_down)
    return (routed + shared).astype(jnp.bfloat16)


def local(
    query_rows,
    key_rows,
    value_rows,
    gate_rows,
    log_decay,
    out_proj,
    moe_input,
    norm_gain,
    routing,
    route_weight,
    expert_gate,
    expert_up,
    expert_down,
    shared_gate,
    shared_up,
    shared_down,
):
    mixer_out = mixer_half(query_rows, key_rows, value_rows, gate_rows, log_decay, out_proj)
    moe_out = moe_half(
        moe_input,
        norm_gain,
        routing,
        route_weight,
        expert_gate,
        expert_up,
        expert_down,
        shared_gate,
        shared_up,
        shared_down,
    )
    return (mixer_out, moe_out)


def solution(mesh):
    split = Mesh(mesh.devices.reshape(4, 4, 2, mesh.shape["tp"]), ("ep_0", "ep_1", "ep_2", "tp"))
    return jax.shard_map(
        local,
        mesh=split,
        in_specs=(
            P(EP, "tp"),
            P(EP, "tp"),
            P(EP, "tp"),
            P(EP, "tp"),
            P("tp", EP),
            P("tp", None),
            P(EP_TP, None),
            P(),
            P(EP_TP, None),
            P(EP_TP, None),
            P(EP_TP, None, None),
            P(EP_TP, None, None),
            P(EP_TP, None, None),
            P(),
            P(),
            P(),
        ),
        out_specs=(P(EP_TP, None), P(EP_TP, None)),
        check_vma=False,
    )
```

profile of v0, /device:TPU:6, one launch (start us, length us, event | category | flops | bytes accessed | tf_op | source)
XLA Modules:
  0.0 366.6 jit_solution(16505537645563051957)
XLA Ops:
  7.2 0.9 copy.93
  8.8 1.2 dynamic-slice
  11.0 2.4 all-reduce
  13.6 10.0 %all-gather.2 = bf16[4,1,2]{2,1,0:T(2,128)(2,1)S(1)} all-gather(bf16[1,1,2]{2,1,0:T(2,128)(2,1)S(1)} %convert_bitcast_fusion.1), channel_id=1, replica_groups=mesh['ep_0'=4,'ep_1'=4,'ep_2'=2,'tp'=4] {'ep_1'}, dimensions={0}, use_global_device_ids=true | all-gather | bytes 20 | tf_op jit(solution)/shard_map/all_gather | solution.py:29
  23.6 11.0 %all-gather.3 = bf16[4,1,2]{2,1,0:T(2,128)(2,1)S(1)} all-gather(bf16[1,1,2]{2,1,0:T(2,128)(2,1)S(1)} %fusion.74), channel_id=1, replica_groups=mesh['ep_0'=4,'ep_1'=4,'ep_2'=2,'tp'=4] {'ep_0'}, dimensions={0}, use_global_device_ids=true | all-gather | bytes 20 | tf_op jit(solution)/shard_map/all_gather | solution.py:29
  35.0 4.0 %reshape.306 = bf16[16,128,2,256]{3,2,1,0:T(2,128)(2,1)} reshape(bf16[2048,512]{1,0:T(8,128)(2,1)} %param.20) | data formatting | bytes 4194304 | tf_op jit(solution)/shard_map/reshape | solution.py:55
  39.1 1.1 reshape.304
  40.2 2.5 copy.58
  42.7 4.6 %fusion.21 = f32[16,2,128,256]{3,2,1,0:T(8,128)} fusion(bf16[16,128,2,256]{3,2,1,0:T(2,128)(2,1)} %reshape.306, bf16[16,128,2,128]{1,3,2,0:T(8,128)(2,1)S(1)} %copy.58, f32[16,128,2]{1,2,0:T(2,128)S(1)} %copy.59), kind=kOutput, calls=%fused_computation.40 | convolution fusion | flops 270008320 | bytes 7356416 | tf_op jit(solution)/shard_map/bmhd,bmhe->bhde/dot_general | solution.py:68
  47.3 28.7 %while.13 = (s32[]{:T(128)}, f32[2,128,256]{2,1,0:T(8,128)S(1)}, f32[16,2,128,256]{3,2,1,0:T(8,128)}, f32[16,2]{1,0:T(8,128)S(1)}, f32[16,2,128,256]{3,2,1,0:T(8,128)}, /*index=5*/s32[]{:T(128)}, s32[]{:T(128)}) while((s32[]{:T(128)}, f32[2,128,256]{2,1,0:T(8,128)S(1)}, f32[16,2,128,256]{3,2,1,0:T(8,128)}, f32[16,2]{1,0:T(8,128)S(1)}, ...), condition=%wide.region_2.3_spmd.clone, body=%wide.region_1.2_spmd.clone.sunk | while | flops 262147 | bytes 1310852 | solution.py:76
  48.0 1.0 bitcast_add_fusion.2
  49.8 1.0 bitcast_add_fusion.2
  51.6 1.0 bitcast_add_fusion.2
  53.4 1.0 bitcast_add_fusion.2
  55.2 1.0 bitcast_add_fusion.2
  57.0 1.0 bitcast_add_fusion.2
  58.8 1.0 bitcast_add_fusion.2
  60.6 1.0 bitcast_add_fusion.2
  62.4 1.0 bitcast_add_fusion.2
  64.2 1.0 bitcast_add_fusion.2
  66.0 1.0 bitcast_add_fusion.2
  67.8 1.0 bitcast_add_fusion.2
  69.6 1.0 bitcast_add_fusion.2
  71.4 1.0 bitcast_add_fusion.2
  73.2 1.0 bitcast_add_fusion.2
  75.0 1.0 bitcast_add_fusion.2
  76.0 2.0 all-gather.1
  78.2 13.4 %all_gather.31 = bf16[4,2,128,256]{3,2,1,0:T(8,128)(2,1)S(1)} all-gather(bf16[1,2,128,256]{3,2,1,0:T(8,128)(2,1)S(1)} %fusion.62), channel_id=1, replica_groups=mesh['ep_0'=4,'ep_1'=4,'ep_2'=2,'tp'=4] {'ep_1'}, dimensions={0}, use_global_device_ids=true | all-gather | bytes 655360 | tf_op jit(solution)/shard_map/all_gather | solution.py:29
  91.8 13.4 %all_gather.32 = bf16[4,2,128,256]{3,2,1,0:T(8,128)(2,1)S(1)} all-gather(bf16[1,2,128,256]{3,2,1,0:T(8,128)(2,1)S(1)} %fusion.61), channel_id=1, replica_groups=mesh['ep_0'=4,'ep_1'=4,'ep_2'=2,'tp'=4] {'ep_0'}, dimensions={0}, use_global_device_ids=true | all-gather | bytes 655360 | tf_op jit(solution)/shard_map/all_gather | solution.py:29
  105.3 2.1 reshape.303
  107.5 5.5 %fusion.23 = f32[16,2,128,256]{3,2,1,0:T(8,128)} fusion(bf16[16,128,2,256]{3,2,1,0:T(2,128)(2,1)} %reshape.306, bf16[16,128,2,128]{1,3,2,0:T(8,128)(2,1)} %copy-done.3, f32[2,16,128]{2,0,1:T(2,128)S(1)} %copy.55, pred[128,128]{1,0:T(8,128)(4,1)S(1)} %iota_compare_fusion.3, bf16[16,128,2,128]{3,2,1,0:T(2,128)(2,1)} %reshape.303), kind=kOutput, calls=%fused_computation.42 | convolution fusion | flops 405798912 | bytes 8421376 | tf_op jit(solution)/shard_map/hbnm,bmhe->bnhe/dot_general | solution.py:65
  114.2 6.7 %fusion.83 = (f32[16,128,2]{1,2,0:T(2,128)S(1)}, f32[16,128,2,256]{3,1,2,0:T(8,128)}) fusion(f32[16,128,2]{1,2,0:T(2,128)S(1)} %copy.66, f32[16,2,128,256]{3,2,1,0:T(8,128)} %get-tuple-element.30, f32[2,128,256]{2,1,0:T(8,128)S(1)} %fusion.53, f32[16,2]{1,0:T(8,128)S(1)} %copy.62, bf16[16,128,2,128]{3,2,1,0:T(2,128)(2,1)S(1)} %copy-done.4, ...), kind=kOutput, calls=%fused_computation.152 | convolution fusion | flops 274722816 | bytes 13926528 | tf_op jit(solution)/shard_map/bnhd,bhde->bnhe/dot_general | solution.py:89
  120.8 5.5 %copy.67 = f32[16,128,2,256]{1,0,3,2:T(8,128)} copy(f32[16,128,2,256]{3,1,2,0:T(8,128)} %get-tuple-element.94) | data formatting | bytes 8388608 | tf_op jit(solution)/shard_map/add | solution.py:96
  126.4 3.9 %copy.52 = bf16[2048,512]{0,1:T(8,128)(2,1)} copy(bf16[2048,512]{1,0:T(8,128)(2,1)} %param.21) | data formatting | bytes 4194304 | tf_op args[3]
  130.3 3.0 multiply_reduce_fusion.1
  133.7 4.1 %fusion.11 = bf16[2048,512]{0,1:T(8,128)(2,1)S(1)} fusion(f32[64,8,16,128]{3,2,1,0:T(8,128)S(1)} %bitcast.170, bf16[2048,512]{0,1:T(8,128)(2,1)} %copy.52, f32[2048,2]{0,1:T(2,128)S(1)} %rsqrt_bitcast_fusion, f32[2048,2]{0,1:T(2,128)S(1)} %get-tuple-element.79), kind=kLoop, calls=%fused_computation.26 | loop fusion | flops 9437184 | bytes 8421376 | tf_op jit(solution)/shard_map/convert_element_type | solution.py:101
  137.9 7.0 %convolution_convert_fusion = bf16[2048,2048]{1,0:T(8,128)(2,1)} fusion(bf16[2048,512]{0,1:T(8,128)(2,1)S(1)} %fusion.11, bf16[512,2048]{1,0:T(8,128)(2,1)S(1)} %copy-done), kind=kOutput, calls=%fused_computation.7 | convolution fusion | flops 4299161600 | bytes 12582912 | tf_op jit(solution)/shard_map/dot_general | solution.py:103
  147.2 13.0 %scatter_custom_fusion = bf16[1024,2048]{1,0:T(8,128)(2,1)} fusion(s32[512]{0:T(512)S(1)} %bitcast.178, bf16[128,2048]{1,0:T(8,128)(2,1)S(1)} %fusion.36, s32[1024]{0:T(1024)S(1)} %pad_clamp_fusion.1, bf16[]{:T(256)} %constant.87.clone.1), kind=kCustom, calls=%fused_computation.32 | custom fusion | bytes 4194306 | tf_op jit(solution)/shard_map/scatter | solution.py:150
  160.3 103.0 %all_to_all.10 = bf16[128,8,2048]{2,1,0:T(8,128)(2,1)S(1)} all-to-all(bf16[128,8,2048]{2,1,0:T(8,128)(2,1)} %bitcast.171), channel_id=1, replica_groups=mesh['ep_0'=4,'ep_1'=4,'ep_2'=2,'tp'=4] {'ep_0','ep_1','ep_2','tp'}, dimensions={0} | all-to-all | bytes 8388608 | tf_op jit(solution)/shard_map/all_to_all | solution.py:155
  263.3 2.0 copy-done.5
  265.2 3.7 %fusion.8 = f32[1024,512]{1,0:T(8,128)} fusion(bf16[128,8,2048]{2,1,0:T(8,128)(2,1)S(1)} %all_to_all.10, bf16[1,2048,512]{2,1,0:T(8,128)(2,1)S(1)} %copy-done.12), kind=kOutput, calls=%fused_computation.18 | convolution fusion | flops 2147483648 | bytes 8388608 | tf_op jit(solution)/shard_map/dot_general | solution.py:111
  268.9 10.6 %convert_bitcast_fusion = bf16[128,8,2048]{2,1,0:T(8,128)(2,1)} fusion(bf16[1,512,2048]{2,1,0:T(8,128)(2,1)} %param.30, f32[1024,512]{1,0:T(8,128)} %fusion.8, bf16[1,2048,512]{2,1,0:T(8,128)(2,1)} %param.29, bf16[128,8,2048]{2,1,0:T(8,128)(2,1)} %copy-done.5), kind=kOutput, calls=%fused_computation.23 | convolution fusion | flops 4300210176 | bytes 14680064 | tf_op jit(solution)/shard_map/dot_general | solution.py:114
  279.5 7.4 %all-to-all-start.1 = ((bf16[128,8,2048]{2,1,0:T(8,128)(2,1)}), bf16[128,8,2048]{2,1,0:T(8,128)(2,1)}, u32[]{:S(2)}, u32[]{:S(2)}) async-start(bf16[128,8,2048]{2,1,0:T(8,128)(2,1)} %convert_bitcast_fusion), calls=%async_computation.2 | async-start | bytes 8388608 | tf_op jit(solution)/shard_map/all_to_all | solution.py:167
  287.6 51.0 %all-to-all-done.1 = bf16[128,8,2048]{2,1,0:T(8,128)(2,1)} async-done(((bf16[128,8,2048]{2,1,0:T(8,128)(2,1)}), bf16[128,8,2048]{2,1,0:T(8,128)(2,1)}, u32[]{:S(2)}, u32[]{:S(2)}) %all-to-all-start.1) | async-done | bytes 4194336 | tf_op jit(solution)/shard_map/all_to_all | solution.py:167
  338.6 7.1 %gather_fusion = bf16[512,2048]{1,0:T(8,128)(2,1)S(1)} fusion(bf16[1024,2048]{1,0:T(8,128)(2,1)} %bitcast.38, s32[1024]{0:T(1024)S(1)} %pad_clamp_fusion), kind=kCustom, calls=%fused_computation.1 | custom fusion | bytes 4196352 | tf_op jit(solution)/shard_map/gather | solution.py:168
  345.7 3.1 reshape.322
  348.8 6.5 %multiply_reduce_fusion = f32[128,2048]{1,0:T(8,128)} fusion(f32[128,4,2048]{2,1,0:T(4,128)} %reshape.322, f32[128,4]{1,0:T(8,128)S(1)} %copy.73), kind=kLoop, calls=%fused_computation.22 | loop fusion | flops 1835008 | bytes 5244928 | tf_op jit(solution)/shard_map/reduce_sum | solution.py:170
  355.3 4.1 %fusion.12 = bf16[128,2048]{1,0:T(8,128)(2,1)} fusion(f32[128,2048]{1,0:T(8,128)} %multiply_reduce_fusion, bf16[512,2048]{1,0:T(8,128)(2,1)} %param.33, bf16[128,2048]{1,0:T(8,128)(2,1)S(1)} %fusion.36, bf16[2048,512]{1,0:T(8,128)(2,1)} %param.32, f32[128,512]{1,0:T(8,128)S(1)} %fusion.84), kind=kOutput, calls=%fused_computation.28 | convolution fusion | flops 537788416 | bytes 6553600 | tf_op jit(solution)/shard_map/dot_general | solution.py:114
  (114 shorter events, 18.3 us)
Async XLA Ops:
  7.2 130.7 %copy-start = (bf16[512,2048]{1,0:T(8,128)(2,1)S(1)}, bf16[512,2048]{1,0:T(8,128)(2,1)}, u32[]{:S(2)}) copy-start(bf16[512,2048]{1,0:T(8,128)(2,1)} %param.23) | copy-start | bytes 6291460
  7.2 352.3 %reduce-scatter.2.cloned.1.call-start = ((), (), s32[]{:S(2)}) async-start(), calls=%async_computation.3 | async-start | bytes 10485760 | tf_op jit(solution)/shard_map/reduce_scatter | solution.py:102
  35.0 4.0 %copy-start.8 = (bf16[2048,256]{1,0:T(8,128)(2,1)S(1)}, bf16[2048,256]{1,0:T(8,128)(2,1)}, u32[]{:S(2)}) copy-start(bf16[2048,256]{1,0:T(8,128)(2,1)} %param.19) | copy-start | bytes 3145732
  42.7 4.6 %copy-start.3 = (bf16[16,128,2,128]{1,3,2,0:T(8,128)(2,1)}, bf16[16,128,2,128]{1,3,2,0:T(8,128)(2,1)S(1)}, u32[]{:S(2)}) copy-start(bf16[16,128,2,128]{1,3,2,0:T(8,128)(2,1)S(1)} %copy.58) | copy-start | bytes 3145732
  113.0 1.2 copy-start.4
  130.3 3.5 copy-start.2
  144.9 0.7 copy-start.10
  145.5 1.3 copy-start.7
  145.6 1.5 copy-start.9
  160.3 105.0 %copy-start.12 = (bf16[1,2048,512]{2,1,0:T(8,128)(2,1)S(1)}, bf16[1,2048,512]{2,1,0:T(8,128)(2,1)}, u32[]{:S(2)}) copy-start(bf16[1,2048,512]{2,1,0:T(8,128)(2,1)} %param.28) | copy-start | bytes 6291460
  263.3 2.0 copy-start.5
  279.5 7.4 %copy-start.11 = (f32[128,4]{0,1:T(4,128)S(1)}, f32[128,4]{0,1:T(4,128)}, u32[]{:S(2)}) copy-start(f32[128,4]{0,1:T(4,128)} %param.27) | copy-start | bytes 6148
  279.5 7.6 %copy-start.6 = (bf16[2048,512]{1,0:T(8,128)(2,1)S(1)}, bf16[2048,512]{1,0:T(8,128)(2,1)}, u32[]{:S(2)}) copy-start(bf16[2048,512]{1,0:T(8,128)(2,1)} %param.31) | copy-start | bytes 6291460
  279.5 59.0 %all-to-all-start.1 = ((bf16[128,8,2048]{2,1,0:T(8,128)(2,1)}), bf16[128,8,2048]{2,1,0:T(8,128)(2,1)}, u32[]{:S(2)}, u32[]{:S(2)}) async-start(bf16[128,8,2048]{2,1,0:T(8,128)(2,1)} %convert_bitcast_fusion), calls=%async_computation.2 | async-start | bytes 8388608 | tf_op jit(solution)/shard_map/all_to_all | solution.py:167
  348.8 10.7 %copy-start.1 = (bf16[512,2048]{1,0:T(8,128)(2,1)S(1)}, bf16[512,2048]{1,0:T(8,128)(2,1)}, u32[]{:S(2)}) copy-start(bf16[512,2048]{1,0:T(8,128)(2,1)} %param.23) | copy-start | bytes 6291460
Sparse Core Ops, SparseCore 0:
  145.0 121.5 reduce-scatter.1
where the time goes:
time: 373 us; the launch traced here: 367 us
  blocking collectives  155 us (42%)
  waiting for transfers between devices  51 us (14%)
  local copies, waits for them, and re-layouts  49.7 us (13%)
  other arithmetic  45 us (12%)
  matrix products  42.6 us (11%)
  between operations  15.3 us (4%)
  starting transfers between devices  7.46 us (2%)
    all_to_all x1, blocking collectives, moe_half(): lax.all_to_all(outgoing.reshape(experts, capacity, model_width), EP_TP, s...  103 us
    all_to_all x1, waiting for transfers between devices, moe_half(): lax.all_to_all(served, EP_TP, split_axis=0, concat_axis=0, tiled=True)  51 us
    all_gather x5, blocking collectives, carried_in(): lax.all_gather(part.astype(kind), axis)  49.8 us
    add x16, other arithmetic, advance(): return (carried_state * shrink_by[:, None, None] + added, carried_state)  16.6 us
    dot_general x2, matrix products, expert_apply(): return jnp.dot(hidden, w_down, preferred_element_type=jnp.float32)  14.7 us
    scatter x1, local copies, waits for them, and re-layouts, moe_half(): outgoing = jnp.zeros((experts * capacity, model_width), jnp.bfloat16).at[...  13 us
    dynamic_update_slice x16, other arithmetic, mixer_half(): lax.scan(advance, jnp.zeros((n_heads, DK, DV), jnp.float32), (jnp.exp(blo...  11.7 us
    unnamed x35, local copies, waits for them, and re-layouts  10.4 us
  transfers between devices with their start and end apart: 2, of which 1 were waited for; matrix products, arithmetic and copies ran while one was open for 14% of the time, Pallas kernels for 0%

commit v1 on v0

v1 whole, which is shorter than its diff:
```python
import functools

import jax
import jax.numpy as jnp
from jax import lax
from jax.experimental import pallas as pl
from jax.experimental.pallas import tpu as pltpu
from jax.sharding import Mesh
from jax.sharding import PartitionSpec as P

DK = 128
DV = 256
BLOCK = 128
EP = ("ep_0", "ep_1", "ep_2")
EP_TP = ("ep_0", "ep_1", "ep_2", "tp")
EPS = 1e-06
MESH = pl.DeviceIdType.MESH
HI = lax.Precision.HIGHEST
F32 = jnp.float32
BF16 = jnp.bfloat16
SCALE = DK ** (-0.5)

NT = (((1,), (1,)), ((), ()))
TN = (((0,), (0,)), ((), ()))


def dot(a, b, dims=None, precision=None):
    if dims is None:
        dims = (((1,), (0,)), ((), ()))
    return lax.dot_general(a, b, dims, precision=precision, preferred_element_type=F32)


def iota(shape, dim):
    return lax.broadcasted_iota(jnp.int32, shape, dim)


def silu(v):
    half = 0.5 * v
    return half * jnp.tanh(half) + half


N_BLK = 16
HEADS = 2
PAY = DK + 16


def mixer_kernel(
    q_ref, k_ref, v_ref, g_ref, ld_ref, wo_ref, out_ref,
    W, R, ret, inner, prev, a_s, c_s, e_s, run, inc, tot_S, tot_f, bef_S, bef_f,
    pay, got_c, got_y, got_z,
    wx_s, wx_r, w1_s, w1_r, w2_s, w2_r, w3_s, w3_r, pre_s, pre_r, ret_s, ret_r, loc_sem,
):
    z = lax.axis_index("ep_0")
    y = lax.axis_index("ep_1")
    c = lax.axis_index("ep_2")
    x = lax.axis_index("tp")
    place = {"ep_0": z, "ep_1": y, "ep_2": c, "tp": x}
    size = {"ep_0": 4, "ep_1": 4, "ep_2": 2, "tp": 4}

    def peer(axis, d):
        return {axis: lax.rem(place[axis] + d, size[axis])}

    links = [(a, d) for a in ("ep_0", "ep_1", "tp") for d in (1, 2, 3)] + [("ep_2", 1)]
    barrier = pltpu.get_barrier_semaphore()
    for a, d in links:
        pl.semaphore_signal(barrier, inc=1, device_id=peer(a, d), device_id_type=MESH)
    pl.semaphore_wait(barrier, len(links))

    def rows(start, n):
        return pl.ds(pl.multiple_of(start, 16), n)

    half0, half1 = pl.ds(0, 1024), pl.ds(1024, 1024)
    r0 = c * 256 + y * 64 + z * 16
    r1 = c * 256 + z * 64 + y * 16

    own_w = pltpu.make_async_copy(wo_ref, W.at[0], loc_sem)
    own_w.start()
    wx = []
    for d in (1, 2, 3):
        for h, (r, cols) in enumerate(((r0, half0), (r1, half1))):
            i = (d - 1) * 2 + h
            cp = pltpu.make_async_remote_copy(
                src_ref=wo_ref.at[rows(r, 16), cols],
                dst_ref=W.at[4 - d, rows(r, 16), cols],
                send_sem=wx_s.at[i],
                recv_sem=wx_r.at[i],
                device_id=peer("tp", d),
                device_id_type=MESH,
            )
            cp.start()
            wx.append(cp)

    for h in range(HEADS):
        for j in range(N_BLK):
            a_s[h * N_BLK + j : h * N_BLK + j + 1, :] = ld_ref[h : h + 1, j * BLOCK : (j + 1) * BLOCK]
    a = a_s[...]
    upper = (iota((BLOCK, BLOCK), 0) <= iota((BLOCK, BLOCK), 1)).astype(F32)
    cum = dot(a, upper, precision=HI)
    c_s[...] = cum
    nb = HEADS * N_BLK
    totb = jnp.broadcast_to(cum[:, BLOCK - 1 : BLOCK], (nb, BLOCK))
    ri, ci = iota((nb, nb), 0), iota((nb, nb), 1)
    same = (ri // N_BLK) == (ci // N_BLK)
    after = dot((same & (ci > ri)).astype(F32), totb, precision=HI)
    e_s[...] = jnp.exp(after + totb - cum) * SCALE
    whole = jnp.exp(after + totb)

    run[...] = jnp.zeros_like(run)

    def col(row):
        return jnp.broadcast_to(row, (BLOCK, BLOCK)).T

    def summary(j, _):
        sl = pl.ds(pl.multiple_of(j * BLOCK, BLOCK), BLOCK)
        for h in range(HEADS):
            kb = k_ref[sl, h * DK : (h + 1) * DK].astype(F32)
            vb = v_ref[sl, h * DV : (h + 1) * DV]
            kd = (kb * col(e_s[pl.ds(h * N_BLK + j, 1), :])).astype(BF16)
            run[h] += dot(kd, vb, TN)
        return 0

    lax.fori_loop(0, N_BLK, summary, 0)
    for h in range(HEADS):
        f = whole[h * N_BLK : h * N_BLK + 1, :]
        tot_f[h] = jnp.concatenate([f, f], axis=1)
        tot_S[h] = run[h]
        bef_S[h] = jnp.zeros((DK, DV), F32)
        bef_f[h] = jnp.ones((1, DV), F32)

    def publish(axis, got, base):
        for h in range(HEADS):
            pay[h, 0:DK, :] = tot_S[h].astype(BF16)
            f = tot_f[h]
            f1 = f.astype(BF16)
            f2 = (f - f1.astype(F32)).astype(BF16)
            row = iota((16, DV), 0)
            top = jnp.where(row == 0, f1.astype(F32), jnp.where(row == 1, f2.astype(F32), 0.0))
            pay[h, DK:PAY, :] = top.astype(BF16)
        cps = []
        for d in range(1, size[axis]):
            cp = pltpu.make_async_remote_copy(
                src_ref=pay,
                dst_ref=got.at[d - 1],
                send_sem=pre_s.at[base + d - 1],
                recv_sem=pre_r.at[base + d - 1],
                device_id=peer(axis, d),
                device_id_type=MESH,
            )
            cp.start()
            cps.append(cp)
        return cps

    def absorb(axis, got, cps):
        n, at = size[axis], place[axis]
        for cp in cps:
            cp.wait()
        for h in range(HEADS):
            sub_f = jnp.ones((1, DV), F32)
            sub_S = jnp.zeros((DK, DV), F32)
            in_f, in_S = sub_f, sub_S
            for k in range(n):
                own = at == k
                slot = jnp.maximum(lax.rem(at - k + n, n) - 1, 0)
                piece = got[slot, h].astype(F32)
                pf = piece[DK : DK + 1, :] + piece[DK + 1 : DK + 2, :]
                pf = jnp.where(own, tot_f[h], pf)
                ps = jnp.where(own, tot_S[h], piece[0:DK, :])
                if k:
                    in_f = jnp.where(own, sub_f, in_f)
                    in_S = jnp.where(own, sub_S, in_S)
                sub_S = pf * sub_S + ps
                sub_f = sub_f * pf
            bef_S[h] = bef_f[h] * in_S + bef_S[h]
            bef_f[h] = bef_f[h] * in_f
            tot_S[h] = sub_S
            tot_f[h] = sub_f

    causal = iota((BLOCK, BLOCK), 0) >= iota((BLOCK, BLOCK), 1)
    run[...] = jnp.zeros_like(run)

    def inside(j, _):
        sl = pl.ds(pl.multiple_of(j * BLOCK, BLOCK), BLOCK)
        for h in range(HEADS):
            qb = q_ref[sl, h * DK : (h + 1) * DK]
            kb = k_ref[sl, h * DK : (h + 1) * DK]
            vb = v_ref[sl, h * DV : (h + 1) * DV]
            crow = c_s[pl.ds(h * N_BLK + j, 1), :]
            ccol = col(crow)
            gap = ccol - jnp.broadcast_to(crow, (BLOCK, BLOCK))
            dec = jnp.exp(jnp.where(causal, gap, -1e30)) * SCALE
            w = (dot(qb, kb, NT) * dec).astype(BF16)
            inner[sl, h * DV : (h + 1) * DV] = dot(w, vb)
            last = crow[:, BLOCK - 1 : BLOCK]
            kd = (kb.astype(F32) * (jnp.exp(last - ccol) * SCALE)).astype(BF16)
            prev[h * N_BLK + j] = run[h]
            run[h] = run[h] * jnp.exp(last) + dot(kd, vb, TN)
        return 0

    cps = publish("ep_2", got_c, 0)
    lax.fori_loop(0, 5, inside, 0)
    absorb("ep_2", got_c, cps)
    cps = publish("ep_1", got_y, 1)
    lax.fori_loop(5, 10, inside, 0)

    for cp in wx:
        cp.wait()

    def spread(axis, d, r, n, cols, ss, rs):
        return pltpu.make_async_remote_copy(
            src_ref=W.at[1:4, rows(r, n), cols],
            dst_ref=W.at[1:4, rows(r, n), cols],
            send_sem=ss,
            recv_sem=rs,
            device_id=peer(axis, d),
            device_id_type=MESH,
        )

    first, first_in = [], []
    for d in (1, 2, 3):
        zf = lax.rem(z + 4 - d, 4)
        yf = lax.rem(y + 4 - d, 4)
        for h, (axis, r, rf, cols) in enumerate(
            (
                ("ep_0", r0, c * 256 + y * 64 + zf * 16, half0),
                ("ep_1", r1, c * 256 + z * 64 + yf * 16, half1),
            )
        ):
            i = (d - 1) * 2 + h
            cp = spread(axis, d, r, 16, cols, w1_s.at[i], w1_r.at[i])
            cp.start()
            first.append(cp)
            first_in.append(spread(axis, d, rf, 16, cols, w1_s.at[i], w1_r.at[i]))

    absorb("ep_1", got_y, cps)
    cps = publish("ep_0", got_z, 4)
    lax.fori_loop(10, N_BLK, inside, 0)
    for cp in first_in:
        cp.wait_recv()

    second, second_in = [], []
    for d in (1, 2, 3):
        zf = lax.rem(z + 4 - d, 4)
        yf = lax.rem(y + 4 - d, 4)
        for h, (axis, r, rf, cols) in enumerate(
            (
                ("ep_1", c * 256 + y * 64, c * 256 + yf * 64, half0),
                ("ep_0", c * 256 + z * 64, c * 256 + zf * 64, half1),
            )
        ):
            i = (d - 1) * 2 + h
            cp = spread(axis, d, r, 64, cols, w2_s.at[i], w2_r.at[i])
            cp.start()
            second.append(cp)
            second_in.append(spread(axis, d, rf, 64, cols, w2_s.at[i], w2_r.at[i]))

    absorb("ep_0", got_z, cps)
    for h in range(HEADS):
        inc[h] = bef_S[h]

    def outer(j, _):
        sl = pl.ds(pl.multiple_of(j * BLOCK, BLOCK), BLOCK)
        for h in range(HEADS):
            qb = q_ref[sl, h * DK : (h + 1) * DK]
            crow = c_s[pl.ds(h * N_BLK + j, 1), :]
            grow = jnp.exp(col(crow))
            grow = jnp.concatenate([grow, grow], axis=1)
            state = inc[h]
            cross = dot(qb, (prev[h * N_BLK + j] + state).astype(BF16))
            inc[h] = state * jnp.exp(crow[:, BLOCK - 1 : BLOCK])
            raw = inner[sl, h * DV : (h + 1) * DV] + cross * grow
            d = raw - jnp.mean(raw, axis=-1, keepdims=True)
            n = d * lax.rsqrt(jnp.mean(d * d, axis=-1, keepdims=True) + EPS)
            gate = silu(g_ref[sl, h * DV : (h + 1) * DV].astype(F32))
            ret[sl, h * DV : (h + 1) * DV] = (gate * n).astype(BF16)
        return 0

    sends = []
    for d in (1, 2, 3, 0):
        p = lax.rem(x + d, 4)
        lax.fori_loop(p * 4, p * 4 + 4, outer, 0) if False else None
    lax.fori_loop(0, N_BLK, outer, 0)
    for d in (1, 2, 3):
        p = lax.rem(x + d, 4)
        cp = pltpu.make_async_remote_copy(
            src_ref=ret.at[rows(p * 512, 512), :],
            dst_ref=R.at[3 - d],
            send_sem=ret_s.at[d - 1],
            recv_sem=ret_r.at[d - 1],
            device_id=peer("tp", d),
            device_id_type=MESH,
        )
        cp.start()
        sends.append(cp)

    for cp in second_in:
        cp.wait_recv()
    own_half = c * 256
    other_half = (1 - c) * 256
    third = spread("ep_2", 1, own_half, 256, pl.ds(0, 2048), w3_s, w3_r)
    third.start()
    third_in = spread("ep_2", 1, other_half, 256, pl.ds(0, 2048), w3_s, w3_r)
    own_w.wait()
    for cp in sends:
        cp.wait_recv()
    third_in.wait_recv()

    def project(t, _):
        cols = pl.ds(pl.multiple_of(t * 512, 512), 512)
        acc = dot(ret[rows(x * 512, 512), :], W[0, :, cols])
        for g in (1, 2, 3):
            acc += dot(R[g - 1], W[g, :, cols])
        out_ref[:, cols] = acc.astype(BF16)
        return 0

    lax.fori_loop(0, 4, project, 0)
    for cp in first + second + sends + [third]:
        cp.wait_send()


def mixer_half(q, k, v, g, ld, wo):
    vm = pl.BlockSpec(memory_space=pltpu.VMEM)
    dma = pltpu.SemaphoreType.DMA
    return pl.pallas_call(
        mixer_kernel,
        name="mixer",
        out_shape=jax.ShapeDtypeStruct((512, 2048), BF16),
        in_specs=[vm, vm, vm, vm, vm, pl.BlockSpec(memory_space=pl.ANY)],
        out_specs=vm,
        scratch_shapes=[
            pltpu.VMEM((4, 512, 2048), BF16),
            pltpu.VMEM((3, 512, 512), BF16),
            pltpu.VMEM((2048, 512), BF16),
            pltpu.VMEM((2048, 512), F32),
            pltpu.VMEM((32, DK, DV), F32),
            pltpu.VMEM((32, BLOCK), F32),
            pltpu.VMEM((32, BLOCK), F32),
            pltpu.VMEM((32, BLOCK), F32),
            pltpu.VMEM((2, DK, DV), F32),
            pltpu.VMEM((2, DK, DV), F32),
            pltpu.VMEM((2, DK, DV), F32),
            pltpu.VMEM((2, 1, DV), F32),
            pltpu.VMEM((2, DK, DV), F32),
            pltpu.VMEM((2, 1, DV), F32),
            pltpu.VMEM((2, PAY, DV), BF16),
            pltpu.VMEM((1, 2, PAY, DV), BF16),
            pltpu.VMEM((3, 2, PAY, DV), BF16),
            pltpu.VMEM((3, 2, PAY, DV), BF16),
            dma((6,)), dma((6,)), dma((6,)), dma((6,)), dma((6,)), dma((6,)), dma, dma,
            dma((7,)), dma((7,)), dma((3,)), dma((3,)), dma,
        ],
        compiler_params=pltpu.CompilerParams(
            collective_id=0, has_side_effects=True, vmem_limit_bytes=50 * 1024 * 1024
        ),
        cost_estimate=pl.CostEstimate(flops=40_000_000_000, bytes_accessed=16_000_000, transcendentals=2_000_000),
    )(q, k, v, g, ld, wo)


SLOTS = 1024
CAP = 8
N_TOK = 128
N_EXP = 128
TOP = 4


def slot_matrix(routing, values=None):
    lane = iota((N_TOK, N_EXP), 1)
    named = jnp.zeros((N_TOK, N_EXP), F32)
    for kk in range(TOP):
        named = named + (routing[:, kk : kk + 1] == lane).astype(F32)
    named = named.astype(BF16)
    lower = (iota((N_TOK, N_TOK), 0) > iota((N_TOK, N_TOK), 1)).astype(BF16)
    rank = dot(lower, named).astype(BF16)
    slot = iota((SLOTS, N_EXP), 0)
    spread = (slot // CAP == iota((SLOTS, N_EXP), 1)).astype(BF16)
    at = (slot % CAP).astype(F32)
    live = (dot(spread, named, NT) > 0.5) & (dot(spread, rank, NT) == at)
    if values is None:
        return live.astype(BF16)
    weight = jnp.zeros((N_TOK, N_EXP), F32)
    for kk in range(TOP):
        weight = weight + jnp.where(routing[:, kk : kk + 1] == lane, values[:, kk : kk + 1], 0.0)
    hi = weight.astype(BF16)
    lo = (weight - hi.astype(F32)).astype(BF16)
    parts = []
    for part in (hi, lo):
        parts.append(jnp.where(live, dot(spread, part, NT), 0.0).astype(BF16))
    return parts


def normed_rows(x_ref, gain_ref):
    v = x_ref[...].astype(F32)
    return (v * lax.rsqrt(jnp.mean(v * v, axis=-1, keepdims=True) + EPS) * gain_ref[...]).astype(BF16)


def dispatch_kernel(x_ref, gain_ref, routing_ref, out_ref, normed_ref):
    normed_ref[...] = normed_rows(x_ref, gain_ref)
    place = slot_matrix(routing_ref[...])
    for t in range(4):
        cols = slice(t * 512, (t + 1) * 512)
        out_ref[:, cols] = dot(place, normed_ref[:, cols]).astype(BF16)


def dispatch(x, gain, routing):
    vm = pl.BlockSpec(memory_space=pltpu.VMEM)
    return pl.pallas_call(
        dispatch_kernel,
        name="dispatch",
        out_shape=(jax.ShapeDtypeStruct((SLOTS, 2048), BF16), jax.ShapeDtypeStruct((N_TOK, 2048), BF16)),
        in_specs=[vm] * 3,
        out_specs=(vm, vm),
        compiler_params=pltpu.CompilerParams(vmem_limit_bytes=32 * 1024 * 1024),
    )(x, gain, routing)


def expert_kernel(rows_ref, wg_ref, wu_ref, wd_ref, out_ref):
    rows = rows_ref[...]
    hidden = (silu(dot(rows, wg_ref[...])) * dot(rows, wu_ref[...])).astype(BF16)
    out_ref[...] = dot(hidden, wd_ref[...]).astype(out_ref.dtype)


def expert(rows, wg, wu, wd, dtype, step):
    n = rows.shape[0]
    whole = lambda w: pl.BlockSpec(w.shape, lambda i: (0, 0))
    return pl.pallas_call(
        expert_kernel,
        name="expert",
        grid=(n // step,),
        out_shape=jax.ShapeDtypeStruct((n, 2048), dtype),
        in_specs=[pl.BlockSpec((step, 2048), lambda i: (i, 0)), whole(wg), whole(wu), whole(wd)],
        out_specs=pl.BlockSpec((step, 2048), lambda i: (i, 0)),
        compiler_params=pltpu.CompilerParams(vmem_limit_bytes=40 * 1024 * 1024),
        cost_estimate=pl.CostEstimate(flops=6 * n * 2048 * 512, bytes_accessed=15_000_000, transcendentals=0),
    )(rows, wg, wu, wd)


def combine_kernel(back_ref, routing_ref, weight_ref, shared_ref, out_ref):
    hi, lo = slot_matrix(routing_ref[...], weight_ref[...])
    for t in range(4):
        cols = slice(t * 512, (t + 1) * 512)
        back = back_ref[:, cols]
        total = dot(hi, back, TN) + dot(lo, back, TN) + shared_ref[:, cols]
        out_ref[:, cols] = total.astype(BF16)


def combine(back, routing, weight, shared):
    vm = pl.BlockSpec(memory_space=pltpu.VMEM)
    return pl.pallas_call(
        combine_kernel,
        name="combine",
        out_shape=jax.ShapeDtypeStruct((N_TOK, 2048), BF16),
        in_specs=[vm] * 4,
        out_specs=vm,
        compiler_params=pltpu.CompilerParams(vmem_limit_bytes=32 * 1024 * 1024),
    )(back, routing, weight, shared)


def local(
    query_rows, key_rows, value_rows, gate_rows, log_decay, out_proj,
    moe_input, norm_gain, routing, route_weight,
    expert_gate, expert_up, expert_down, shared_gate, shared_up, shared_down,
):
    slots, normed = dispatch(moe_input, norm_gain.reshape(1, -1), routing)
    exchange = lambda r: lax.all_to_all(
        r.reshape(N_EXP, CAP, 2048), EP_TP, split_axis=0, concat_axis=0, tiled=True
    ).reshape(SLOTS, 2048)
    received = exchange(slots)
    mixer_out = mixer_half(query_rows, key_rows, value_rows, gate_rows, log_decay, out_proj)
    served = expert(received, expert_gate[0], expert_up[0], expert_down[0], BF16, 256)
    returned = exchange(served)
    shared = expert(normed, shared_gate, shared_up, shared_down, F32, 128)
    moe_out = combine(returned, routing, route_weight, shared)
    return (mixer_out, moe_out)


def solution(mesh):
    split = Mesh(mesh.devices.reshape(4, 4, 2, mesh.shape["tp"]), ("ep_0", "ep_1", "ep_2", "tp"))
    return jax.shard_map(
        local,
        mesh=split,
        in_specs=(
            P(EP, "tp"),
            P(EP, "tp"),
            P(EP, "tp"),
            P(EP, "tp"),
            P("tp", EP),
            P("tp", None),
            P(EP_TP, None),
            P(),
            P(EP_TP, None),
            P(EP_TP, None),
            P(EP_TP, None, None),
            P(EP_TP, None, None),
            P(EP_TP, None, None),
            P(),
            P(),
            P(),
        ),
        out_specs=(P(EP_TP, None), P(EP_TP, None)),
        check_vma=False,
    )
```

time: 373 us -> 196 us (0.53); the launches traced: 367 us -> 194 us
  Pallas kernels: 0 us -> 118 us
  blocking collectives: 155 us -> 62.4 us
  waiting for transfers between devices: 51 us -> 0.01 us
  other arithmetic: 45 us -> 0 us
  local copies, waits for them, and re-layouts: 49.7 us -> 5.98 us
  matrix products: 42.6 us -> 0 us
  between operations: 15.3 us -> 0.8 us
    pallas_call x0 -> x5, Pallas kernels: none -> 118 us  [the longest x1 101 us: mixer_half(): pl.pallas_call(mixer_kernel, name='mixer', out_shape=jax.ShapeDtypeStruct...]
    all_to_all x1, waiting for transfers between devices: 51 us -> 0.01 us  [local(): lax.all_to_all(r.reshape(N_EXP, CAP, 2048), EP_TP, split_axis=0, concat_a...]
    all_gather x5 -> x0, blocking collectives: 49.8 us -> none  [carried_in(): lax.all_gather(part.astype(kind), axis)]
    dot_general x8 -> x0, matrix products: 42.6 us -> none  [the longest x2 14.7 us: expert_apply(): return jnp.dot(hidden, w_down, preferred_element_type=jnp.float32)]
    all_to_all x1, blocking collectives: 103 us -> 62.4 us  [local(): lax.all_to_all(r.reshape(N_EXP, CAP, 2048), EP_TP, split_axis=0, concat_a...]
    add x16 -> x0, other arithmetic: 16.6 us -> none  [advance(): return (carried_state * shrink_by[:, None, None] + added, carried_state)]
    scatter x1 -> x0, local copies, waits for them, and re-layouts: 13 us -> none  [moe_half(): outgoing = jnp.zeros((experts * capacity, model_width), jnp.bfloat16).at[...]
    dynamic_update_slice x16 -> x0, other arithmetic: 11.7 us -> none  [mixer_half(): lax.scan(advance, jnp.zeros((n_heads, DK, DV), jnp.float32), (jnp.exp(blo...]
  transfers between devices with their start and end apart: 2 -> 1, of which waited for: 1 -> 0; matrix products, arithmetic and copies ran while one was open for 14% -> 0% of each run, Pallas kernels for 0% -> 53%
where the time goes in v1:
time: 196 us; the launch traced here: 194 us
  Pallas kernels  118 us (60%)
  blocking collectives  62.4 us (32%)
  starting transfers between devices  6.54 us (3%)
  local copies, waits for them, and re-layouts  5.98 us (3%)
    pallas_call x1, Pallas kernels, mixer_half(): pl.pallas_call(mixer_kernel, name='mixer', out_shape=jax.ShapeDtypeStruct...  101 us
    all_to_all x1, blocking collectives, local(): lax.all_to_all(r.reshape(N_EXP, CAP, 2048), EP_TP, split_axis=0, concat_a...  62.4 us
    pallas_call x2, Pallas kernels, expert(): pl.pallas_call(expert_kernel, name='expert', grid=(n // step,), out_shape...  9.9 us
    all_to_all x1, starting transfers between devices, local(): lax.all_to_all(r.reshape(N_EXP, CAP, 2048), EP_TP, split_axis=0, concat_a...  6.54 us
    unnamed x31, local copies, waits for them, and re-layouts  5.98 us
    pallas_call x1, Pallas kernels, combine(): pl.pallas_call(combine_kernel, name='combine', out_shape=jax.ShapeDtypeSt...  5.08 us
  transfers between devices with their start and end apart: 1, of which 0 were waited for; matrix products, arithmetic and copies ran while one was open for 0% of the time, Pallas kernels for 53%

profile of v1, /device:TPU:6, one launch (start us, length us, event | category | flops | bytes accessed | tf_op | source)
XLA Modules:
  0.0 193.8 jit_solution(15686282305327752493)
XLA Ops:
  0.6 0.8 copy.18.routing_ref
  1.4 0.0 copy-start.4
  1.4 1.0 copy-done.4
  2.5 0.0 copy-start.5
  2.5 0.7 copy-done.5
  3.2 1.7 dispatch.1
  4.8 0.0 copy-start.6
  4.9 0.0 copy-start.7
  4.9 0.0 copy-start.8
  4.9 62.4 %all_to_all.10 = bf16[128,8,2048]{2,1,0:T(8,128)(2,1)} all-to-all(bf16[128,8,2048]{2,1,0:T(8,128)(2,1)S(1)} %bitcast.9), channel_id=1, replica_groups=mesh['ep_0'=4,'ep_1'=4,'ep_2'=2,'tp'=4] {'ep_0','ep_1','ep_2','tp'}, dimensions={0} | all-to-all | bytes 8388608 | tf_op jit(solution)/shard_map/all_to_all | solution.py:463
  67.3 0.0 copy-done.6
  67.3 0.0 copy-done.7
  67.3 0.0 copy-done.8
  67.3 8.8 %expert.2 = bf16[1024,2048]{1,0:T(8,128)(2,1)S(1)} custom-call(bf16[1024,2048]{1,0:T(8,128)(2,1)} %bitcast.14, bf16[2048,512]{1,0:T(8,128)(2,1)S(1)} %bitcast.11, bf16[2048,512]{1,0:T(8,128)(2,1)S(1)} %bitcast.12, bf16[512,2048]{1,0:T(8,128)(2,1)S(1)} %bitcast.13), custom_call_target="tpu_custom_call" | custom-call | flops 6442450944 | bytes 15000000 | tf_op jit(solution)/shard_map/expert/pallas_call | solution.py:424
  76.1 0.0 copy-start
  76.2 2.0 %copy-done = bf16[1024,2048]{1,0:T(8,128)(2,1)} copy-done((bf16[1024,2048]{1,0:T(8,128)(2,1)}, bf16[1024,2048]{1,0:T(8,128)(2,1)S(1)}, u32[]{:S(2)}) %copy-start) | copy-done | bytes 4194328
  78.1 0.0 copy-start.13
  78.1 0.0 copy-start.9
  78.1 0.0 copy-start.10
  78.1 0.0 copy-start.11
  78.1 6.5 %all-to-all-start.1 = ((bf16[128,8,2048]{2,1,0:T(8,128)(2,1)}), bf16[128,8,2048]{2,1,0:T(8,128)(2,1)}, u32[]{:S(2)}, u32[]{:S(2)}) async-start(bf16[128,8,2048]{2,1,0:T(8,128)(2,1)} %bitcast.8), calls=%async_computation.1 | async-start | bytes 8388608 | tf_op jit(solution)/shard_map/all_to_all | solution.py:463
  84.7 0.0 copy-done.13
  84.7 0.1 copy.20.weight_ref
  84.8 0.0 copy-done.9
  84.8 0.0 copy-done.10
  84.8 0.0 copy-done.11
  84.8 0.0 copy-start.1
  84.8 0.0 copy-start.2
  84.9 0.0 copy-start.3
  84.9 101.4 %mixer.1 = bf16[512,2048]{1,0:T(8,128)(2,1)} custom-call(bf16[2048,256]{1,0:T(8,128)(2,1)S(1)} %copy-done.9, bf16[2048,256]{1,0:T(8,128)(2,1)S(1)} %copy-done.10, bf16[2048,512]{1,0:T(8,128)(2,1)} %v_ref.1, bf16[2048,512]{1,0:T(8,128)(2,1)} %g_ref.1, f32[2,2048]{1,0:T(2,128)S(1)} %copy-done.11, bf16[512,2048]{1,0:T(8,128)(2,1)} %wo_ref.1), custom_call_target="tpu_custom_call" | custom-call | flops 40000000000 | bytes 16000000 | tf_op jit(solution)/shard_map/mixer/pallas_call | solution.py:323
  186.3 0.0 copy-done.1
  186.3 0.0 copy-done.2
  186.3 0.0 copy-done.3
  186.3 1.1 expert.3.shared_ref
  187.4 0.0 all-to-all-done.1
  187.4 0.0 copy-start.12
  187.4 5.1 %combine.1 = bf16[128,2048]{1,0:T(8,128)(2,1)} custom-call(bf16[1024,2048]{1,0:T(8,128)(2,1)} %bitcast.7.back_ref, s32[128,4]{1,0:T(8,128)S(1)} %copy.18.routing_ref, f32[128,4]{1,0:T(8,128)S(1)} %copy.20.weight_ref, f32[128,2048]{1,0:T(8,128)S(1)} %expert.3.shared_ref), custom_call_target="tpu_custom_call" | custom-call | tf_op jit(solution)/shard_map/combine/pallas_call | solution.py:447
  192.5 0.0 copy-done.12
  192.5 1.3 copy.22
Async XLA Ops:
  1.4 1.0 copy-start.4
  2.5 0.7 copy-start.5
  4.8 62.5 %copy-start.6 = (bf16[1,2048,512]{2,1,0:T(8,128)(2,1)S(1)}, bf16[1,2048,512]{2,1,0:T(8,128)(2,1)}, u32[]{:S(2)}) copy-start(bf16[1,2048,512]{2,1,0:T(8,128)(2,1)} %param.26) | copy-start | bytes 6291460
  4.9 62.5 %copy-start.7 = (bf16[1,2048,512]{2,1,0:T(8,128)(2,1)S(1)}, bf16[1,2048,512]{2,1,0:T(8,128)(2,1)}, u32[]{:S(2)}) copy-start(bf16[1,2048,512]{2,1,0:T(8,128)(2,1)} %param.27) | copy-start | bytes 6291460
  4.9 62.5 %copy-start.8 = (bf16[1,512,2048]{2,1,0:T(8,128)(2,1)S(1)}, bf16[1,512,2048]{2,1,0:T(8,128)(2,1)}, u32[]{:S(2)}) copy-start(bf16[1,512,2048]{2,1,0:T(8,128)(2,1)} %param.28) | copy-start | bytes 6291460
  76.1 2.0 %copy-start = (bf16[1024,2048]{1,0:T(8,128)(2,1)}, bf16[1024,2048]{1,0:T(8,128)(2,1)S(1)}, u32[]{:S(2)}) copy-start(bf16[1024,2048]{1,0:T(8,128)(2,1)S(1)} %expert.2) | copy-start | bytes 12582916
  78.1 6.6 %copy-start.13 = (f32[128,4]{0,1:T(4,128)S(1)}, f32[128,4]{0,1:T(4,128)}, u32[]{:S(2)}) copy-start(f32[128,4]{0,1:T(4,128)} %param.25) | copy-start | bytes 6148
  78.1 6.7 %copy-start.9 = (bf16[2048,256]{1,0:T(8,128)(2,1)S(1)}, bf16[2048,256]{1,0:T(8,128)(2,1)}, u32[]{:S(2)}) copy-start(bf16[2048,256]{1,0:T(8,128)(2,1)} %q_ref.1) | copy-start | bytes 3145732
  78.1 6.7 %copy-start.10 = (bf16[2048,256]{1,0:T(8,128)(2,1)S(1)}, bf16[2048,256]{1,0:T(8,128)(2,1)}, u32[]{:S(2)}) copy-start(bf16[2048,256]{1,0:T(8,128)(2,1)} %k_ref.1) | copy-start | bytes 3145732
  78.1 6.7 %copy-start.11 = (f32[2,2048]{1,0:T(2,128)S(1)}, f32[2,2048]{1,0:T(2,128)}, u32[]{:S(2)}) copy-start(f32[2,2048]{1,0:T(2,128)} %ld_ref.1) | copy-start | bytes 49156
  78.1 109.3 %all-to-all-start.1 = ((bf16[128,8,2048]{2,1,0:T(8,128)(2,1)}), bf16[128,8,2048]{2,1,0:T(8,128)(2,1)}, u32[]{:S(2)}, u32[]{:S(2)}) async-start(bf16[128,8,2048]{2,1,0:T(8,128)(2,1)} %bitcast.8), calls=%async_computation.1 | async-start | bytes 8388608 | tf_op jit(solution)/shard_map/all_to_all | solution.py:463
  84.8 101.4 %copy-start.1 = (bf16[2048,512]{1,0:T(8,128)(2,1)S(1)}, bf16[2048,512]{1,0:T(8,128)(2,1)}, u32[]{:S(2)}) copy-start(bf16[2048,512]{1,0:T(8,128)(2,1)} %wg_ref.1) | copy-start | bytes 6291460
  84.8 101.4 %copy-start.2 = (bf16[2048,512]{1,0:T(8,128)(2,1)S(1)}, bf16[2048,512]{1,0:T(8,128)(2,1)}, u32[]{:S(2)}) copy-start(bf16[2048,512]{1,0:T(8,128)(2,1)} %wu_ref.1) | copy-start | bytes 6291460
  84.9 101.4 %copy-start.3 = (bf16[512,2048]{1,0:T(8,128)(2,1)S(1)}, bf16[512,2048]{1,0:T(8,128)(2,1)}, u32[]{:S(2)}) copy-start(bf16[512,2048]{1,0:T(8,128)(2,1)} %wd_ref.1) | copy-start | bytes 6291460
  187.4 5.1 %copy-start.12 = (bf16[512,2048]{1,0:T(8,128)(2,1)S(1)}, bf16[512,2048]{1,0:T(8,128)(2,1)}, u32[]{:S(2)}) copy-start(bf16[512,2048]{1,0:T(8,128)(2,1)} %mixer.1) | copy-start | bytes 6291460

commit v2 on v1

--- a/solution.py
+++ b/solution.py
@@ -275,9 +275,6 @@
         return 0
 
     sends = []
-    for d in (1, 2, 3, 0):
-        p = lax.rem(x + d, 4)
-        lax.fori_loop(p * 4, p * 4 + 4, outer, 0) if False else None
     lax.fori_loop(0, N_BLK, outer, 0)
     for d in (1, 2, 3):
         p = lax.rem(x + d, 4)
@@ -355,103 +352,313 @@
     )(q, k, v, g, ld, wo)
 
 
-SLOTS = 1024
+N_TOK = 128
+TOP = 4
 CAP = 8
-N_TOK = 128
-N_EXP = 128
-TOP = 4
-
-
-def slot_matrix(routing, values=None):
-    lane = iota((N_TOK, N_EXP), 1)
-    named = jnp.zeros((N_TOK, N_EXP), F32)
-    for kk in range(TOP):
-        named = named + (routing[:, kk : kk + 1] == lane).astype(F32)
-    named = named.astype(BF16)
-    lower = (iota((N_TOK, N_TOK), 0) > iota((N_TOK, N_TOK), 1)).astype(BF16)
-    rank = dot(lower, named).astype(BF16)
-    slot = iota((SLOTS, N_EXP), 0)
-    spread = (slot // CAP == iota((SLOTS, N_EXP), 1)).astype(BF16)
-    at = (slot % CAP).astype(F32)
-    live = (dot(spread, named, NT) > 0.5) & (dot(spread, rank, NT) == at)
-    if values is None:
-        return live.astype(BF16)
-    weight = jnp.zeros((N_TOK, N_EXP), F32)
-    for kk in range(TOP):
-        weight = weight + jnp.where(routing[:, kk : kk + 1] == lane, values[:, kk : kk + 1], 0.0)
-    hi = weight.astype(BF16)
-    lo = (weight - hi.astype(F32)).astype(BF16)
-    parts = []
-    for part in (hi, lo):
-        parts.append(jnp.where(live, dot(spread, part, NT), 0.0).astype(BF16))
-    return parts
-
-
-def normed_rows(x_ref, gain_ref):
+N_EP = 32
+ROWS = N_EP * CAP
+HALF = 1024
+
+
+def moe_steps(ctx, x_ref, gain_ref, meta_ref, wg_hbm, wu_hbm, wd_hbm, sg_hbm, su_hbm, sd_hbm, out_ref, s):
+    z, y, c, x = ctx.z, ctx.y, ctx.c, ctx.x
+    start, mod = ctx.start, ctx.mod
+
+    loads = []
+    for i, (src, dst) in enumerate(
+        ((sg_hbm, s.sg), (su_hbm, s.su), (sd_hbm, s.sd), (wg_hbm.at[0], s.wg), (wu_hbm.at[0], s.wu), (wd_hbm.at[0], s.wd))
+    ):
+        cp = pltpu.make_async_copy(src, dst, s.load.at[i])
+        cp.start()
+        loads.append(cp)
+
     v = x_ref[...].astype(F32)
-    return (v * lax.rsqrt(jnp.mean(v * v, axis=-1, keepdims=True) + EPS) * gain_ref[...]).astype(BF16)
-
-
-def dispatch_kernel(x_ref, gain_ref, routing_ref, out_ref, normed_ref):
-    normed_ref[...] = normed_rows(x_ref, gain_ref)
-    place = slot_matrix(routing_ref[...])
-    for t in range(4):
-        cols = slice(t * 512, (t + 1) * 512)
-        out_ref[:, cols] = dot(place, normed_ref[:, cols]).astype(BF16)
-
-
-def dispatch(x, gain, routing):
+    s.X[0] = (v * lax.rsqrt(jnp.mean(v * v, axis=-1, keepdims=True) + EPS) * gain_ref[...]).astype(BF16)
+    s.meta[0] = meta_ref[...]
+    gathers = {}
+    sends = []
+    for d in (1, 3, 2):
+        a = start(s.meta.at[0], s.meta.at[4 - d], s.gm_s.at[d - 1], s.gm_r.at[d - 1], tp=d)
+        b = start(s.X.at[0], s.X.at[4 - d], s.gx_s.at[d - 1], s.gx_r.at[d - 1], tp=d)
+        gathers[4 - d] = (a, b)
+        sends += [a, b]
+
+    def build(gg):
+        if gg:
+            for cp in gathers[gg]:
+                cp.wait_recv()
+        rt = s.meta[gg, 0:TOP, :]
+        wt = s.meta[gg, TOP : 2 * TOP, :]
+        ident = (iota((N_EP, N_TOK), 0) * 4 + x).astype(F32)
+        named = jnp.zeros((N_EP, N_TOK), F32)
+        weight = jnp.zeros((N_EP, N_TOK), F32)
+        for kk in range(TOP):
+            hit = rt[kk : kk + 1, :] == ident
+            named = named + jnp.where(hit, 1.0, 0.0)
+            weight = weight + jnp.where(hit, wt[kk : kk + 1, :], 0.0)
+        named = named.astype(BF16)
+        earlier = (iota((N_TOK, N_TOK), 0) < iota((N_TOK, N_TOK), 1)).astype(F32).astype(BF16)
+        rank = dot(named, earlier).astype(BF16)
+        slot = iota((ROWS, N_EP), 0)
+        spread = (slot // CAP == iota((ROWS, N_EP), 1)).astype(F32).astype(BF16)
+        at = (iota((ROWS, N_TOK), 0) % CAP).astype(F32)
+        live = (dot(spread, named) > 0.5) & (dot(spread, rank) == at)
+        hi = weight.astype(BF16)
+        lo = (weight - hi.astype(F32)).astype(BF16)
+        s.whi[gg] = jnp.where(live, dot(spread, hi), 0.0).astype(BF16)
+        s.wlo[gg] = jnp.where(live, dot(spread, lo), 0.0).astype(BF16)
+        place = jnp.where(live, 1.0, 0.0).astype(BF16)
+        for h in range(2):
+            rows = dot(place, s.X[gg, :, h * HALF : (h + 1) * HALF]).astype(BF16)
+            s.D[gg, h] = rows.reshape(4, 4, 2, CAP, HALF)
+        s.M[gg, 0, z] = s.D[gg, 0, z]
+        for zz in range(4):
+            s.M[gg, 1, y, zz] = s.D[gg, 1, zz, y]
+        for d in (1, 3, 2):
+            zp, yp = mod(z + d), mod(y + d)
+            first[gg, 0].append(
+                start(s.D.at[gg, 0, zp], s.M.at[gg, 0, z], s.a_s.at[gg, 0, d - 1], s.a_r.at[gg, 0, d - 1], ep_0=d)
+            )
+            first[gg, 1].append(
+                start(s.D.at[gg, 1, :, yp], s.M.at[gg, 1, y], s.a_s.at[gg, 1, d - 1], s.a_r.at[gg, 1, d - 1], ep_1=d)
+            )
+
+    first = {(gg, h): [] for gg in range(4) for h in range(2)}
+    second = {(gg, h): [] for gg in range(4) for h in range(2)}
+    third = {(gg, h): [] for gg in range(4) for h in range(2)}
+    fourth = {(gg, h): [] for gg in range(4) for h in range(2)}
+    hops = [(1, 0), (3, 0), (1, 1), (3, 1), (2, 0), (2, 1), (0, 1)]
+
+    def relay(gg):
+        for h in range(2):
+            for cp in first[gg, h]:
+                cp.wait_recv()
+            for i, (d, e) in enumerate(hops):
+                zp, yp, cp_ = mod(z + d), mod(y + d), lax.rem(c + e, 2)
+                if h == 0:
+                    src, dst = s.M.at[gg, 0, :, yp, cp_], s.V.at[gg, 0, :, y, c]
+                    to = {"ep_1": d, "ep_2": e}
+                else:
+                    src, dst = s.M.at[gg, 1, :, zp, cp_], s.V.at[gg, 1, z, :, c]
+                    to = {"ep_0": d, "ep_2": e}
+                second[gg, h].append(start(src, dst, s.b_s.at[gg, h, i], s.b_r.at[gg, h, i], **to))
+            for k in range(4):
+                if h == 0:
+                    s.V[gg, 0, k, y, c] = s.M[gg, 0, k, y, c]
+                else:
+                    s.V[gg, 1, z, k, c] = s.M[gg, 1, k, z, c]
+
+    def expert(gg):
+        for h in range(2):
+            for cp in second[gg, h]:
+                cp.wait_recv()
+        a = s.V[gg, 0].reshape(ROWS, HALF)
+        b = s.V[gg, 1].reshape(ROWS, HALF)
+        gate = dot(a, s.wg[0:HALF]) + dot(b, s.wg[HALF:])
+        up = dot(a, s.wu[0:HALF]) + dot(b, s.wu[HALF:])
+        hidden = (silu(gate) * up).astype(BF16)
+        for h in range(2):
+            rows = dot(hidden, s.wd[:, h * HALF : (h + 1) * HALF]).astype(BF16)
+            s.V[gg, h] = rows.reshape(4, 4, 2, CAP, HALF)
+
+    def give_back(gg):
+        for h in range(2):
+            for i, (d, e) in enumerate(hops):
+                zp, yp, cp_ = mod(z + d), mod(y + d), lax.rem(c + e, 2)
+                if h == 0:
+                    src, dst = s.V.at[gg, 0, :, yp, cp_], s.N.at[gg, 0, :, y, c]
+                    to = {"ep_1": d, "ep_2": e}
+                else:
+                    src, dst = s.V.at[gg, 1, zp, :, cp_], s.N.at[gg, 1, :, z, c]
+                    to = {"ep_0": d, "ep_2": e}
+                third[gg, h].append(start(src, dst, s.c_s.at[gg, h, i], s.c_r.at[gg, h, i], **to))
+            for k in range(4):
+                if h == 0:
+                    s.N[gg, 0, k, y, c] = s.V[gg, 0, k, y, c]
+                else:
+                    s.N[gg, 1, k, z, c] = s.V[gg, 1, z, k, c]
+
+    def relay_back(gg):
+        for h in range(2):
+            for cp in third[gg, h]:
+                cp.wait_recv()
+            for d in (1, 3, 2):
+                zp, yp = mod(z + d), mod(y + d)
+                if h == 0:
+                    cp = start(s.N.at[gg, 0, zp], s.B.at[gg, 0, z], s.d_s.at[gg, 0, d - 1], s.d_r.at[gg, 0, d - 1], ep_0=d)
+                else:
+                    cp = start(s.N.at[gg, 1, yp], s.B.at[gg, 1, :, y], s.d_s.at[gg, 1, d - 1], s.d_r.at[gg, 1, d - 1], ep_1=d)
+                fourth[gg, h].append(cp)
+            if h == 0:
+                s.B[gg, 0, z] = s.N[gg, 0, z]
+            else:
+                for zz in range(4):
+                    s.B[gg, 1, zz, y] = s.N[gg, 1, y, zz]
+
+    reduces = {}
+
+    def fold(gg):
+        for h in range(2):
+            cols = slice(h * HALF, (h + 1) * HALF)
+            for cp in fourth[gg, h]:
+                cp.wait_recv()
+            back = s.B[gg, h].reshape(ROWS, HALF)
+            part = dot(s.whi[gg], back, TN) + dot(s.wlo[gg], back, TN)
+            if gg == 0:
+                s.acc[:, cols] = s.acc[:, cols] + part
+            else:
+                s.P[gg - 1, h] = part.astype(BF16)
+                reduces[gg, h] = start(
+                    s.P.at[gg - 1, h], s.G.at[gg - 1, h], s.e_s.at[gg - 1, h], s.e_r.at[gg - 1, h], tp=gg
+                )
+
+    def shared():
+        for cp in loads[:3]:
+            cp.wait()
+        rows = s.X[0]
+        hidden = (silu(dot(rows, s.sg[...])) * dot(rows, s.su[...])).astype(BF16)
+        for h in range(2):
+            cols = slice(h * HALF, (h + 1) * HALF)
+            s.acc[:, cols] = dot(hidden, s.sd[:, cols])
+
+    def finish():
+        for h in range(2):
+            cols = slice(h * HALF, (h + 1) * HALF)
+            total = s.acc[:, cols]
+            for gg in (1, 2, 3):
+                reduces[gg, h].wait_recv()
+                total = total + s.G[gg - 1, h].astype(F32)
+            out_ref[:, cols] = total.astype(BF16)
+        for group in (first, second, third, fourth):
+            for cps in group.values():
+                for cp in cps:
+                    cp.wait_send()
+        for cp in list(reduces.values()) + sends:
+            cp.wait_send()
+
+    def weights():
+        for cp in loads[3:]:
+            cp.wait()
+
+    return dict(
+        build=build, relay=relay, expert=expert, give_back=give_back, relay_back=relay_back,
+        fold=fold, shared=shared, finish=finish, weights=weights,
+    )
+
+
+class Names:
+    pass
+
+
+class Ctx:
+    def __init__(self):
+        self.z = lax.axis_index("ep_0")
+        self.y = lax.axis_index("ep_1")
+        self.c = lax.axis_index("ep_2")
+        self.x = lax.axis_index("tp")
+        self.place = {"ep_0": self.z, "ep_1": self.y, "ep_2": self.c, "tp": self.x}
+        self.size = {"ep_0": 4, "ep_1": 4, "ep_2": 2, "tp": 4}
+
+    def mod(self, v):
+        return lax.rem(v, 4)
+
+    def peer(self, **offsets):
+        return {a: lax.rem(self.place[a] + d, self.size[a]) for a, d in offsets.items() if d}
+
+    def copy(self, src, dst, send, recv, **offsets):
+        return pltpu.make_async_remote_copy(
+            src_ref=src, dst_ref=dst, send_sem=send, recv_sem=recv,
+            device_id=self.peer(**offsets), device_id_type=MESH,
+        )
+
+    def start(self, src, dst, send, recv, **offsets):
+        cp = self.copy(src, dst, send, recv, **offsets)
+        cp.start()
+        return cp
+
+
+def greet(ctx):
+    peers = [dict(tp=d) for d in (1, 2, 3)]
+    peers += [dict(ep_0=d, ep_2=e) for d in (1, 2, 3) for e in (0, 1)]
+    peers += [dict(ep_1=d, ep_2=e) for d in (1, 2, 3) for e in (0, 1)]
+    peers += [dict(ep_2=1)]
+    barrier = pltpu.get_barrier_semaphore()
+    for p in peers:
+        pl.semaphore_signal(barrier, inc=1, device_id=ctx.peer(**p), device_id_type=MESH)
+    pl.semaphore_wait(barrier, len(peers))
+
+
+DMA = pltpu.SemaphoreType.DMA
+BLK = (4, 4, 2, CAP, HALF)
+MOE_SCRATCH = dict(
+    sg=pltpu.VMEM((2048, 512), BF16), su=pltpu.VMEM((2048, 512), BF16), sd=pltpu.VMEM((512, 2048), BF16),
+    wg=pltpu.VMEM((2048, 512), BF16), wu=pltpu.VMEM((2048, 512), BF16), wd=pltpu.VMEM((512, 2048), BF16),
+    X=pltpu.VMEM((4, N_TOK, 2048), BF16), meta=pltpu.VMEM((4, 8, N_TOK), F32),
+    whi=pltpu.VMEM((4, ROWS, N_TOK), BF16), wlo=pltpu.VMEM((4, ROWS, N_TOK), BF16),
+    D=pltpu.VMEM((4, 2) + BLK, BF16), M=pltpu.VMEM((4, 2) + BLK, BF16), V=pltpu.VMEM((4, 2) + BLK, BF16),
+    N=pltpu.VMEM((4, 2) + BLK, BF16), B=pltpu.VMEM((4, 2) + BLK, BF16),
+    acc=pltpu.VMEM((N_TOK, 2048), F32),
+    P=pltpu.VMEM((3, 2, N_TOK, HALF), BF16), G=pltpu.VMEM((3, 2, N_TOK, HALF), BF16),
+    load=DMA((6,)),
+    gm_s=DMA((3,)), gm_r=DMA((3,)), gx_s=DMA((3,)), gx_r=DMA((3,)),
+    a_s=DMA((4, 2, 3)), a_r=DMA((4, 2, 3)), b_s=DMA((4, 2, 7)), b_r=DMA((4, 2, 7)),
+    c_s=DMA((4, 2, 7)), c_r=DMA((4, 2, 7)), d_s=DMA((4, 2, 3)), d_r=DMA((4, 2, 3)),
+    e_s=DMA((3, 2)), e_r=DMA((3, 2)),
+)
+
+
+def moe_kernel(x_ref, gain_ref, meta_ref, wg, wu, wd, sg, su, sd, out_ref, *scratch):
+    ctx = Ctx()
+    s = Names()
+    for name, ref in zip(MOE_SCRATCH, scratch):
+        setattr(s, name, ref)
+    greet(ctx)
+    m = moe_steps(ctx, x_ref, gain_ref, meta_ref, wg, wu, wd, sg, su, sd, out_ref, s)
+    m["build"](0)
+    m["shared"]()
+    m["build"](1)
+    m["relay"](0)
+    m["build"](3)
+    m["relay"](1)
+    m["weights"]()
+    m["expert"](0)
+    m["build"](2)
+    m["relay"](3)
+    m["expert"](1)
+    m["give_back"](1)
+    m["relay"](2)
+    m["expert"](3)
+    m["give_back"](3)
+    m["relay_back"](1)
+    m["expert"](2)
+    m["give_back"](2)
+    m["relay_back"](3)
+    m["give_back"](0)
+    m["fold"](1)
+    m["relay_back"](2)
+    m["fold"](3)
+    m["relay_back"](0)
+    m["fold"](2)
+    m["fold"](0)
+    m["finish"]()
+
+
+def moe_half(x, gain, routing, weight, wg, wu, wd, sg, su, sd):
+    meta = jnp.concatenate([routing.T.astype(F32), weight.T], axis=0)
     vm = pl.BlockSpec(memory_space=pltpu.VMEM)
+    hbm = pl.BlockSpec(memory_space=pl.ANY)
     return pl.pallas_call(
-        dispatch_kernel,
-        name="dispatch",
-        out_shape=(jax.ShapeDtypeStruct((SLOTS, 2048), BF16), jax.ShapeDtypeStruct((N_TOK, 2048), BF16)),
-        in_specs=[vm] * 3,
-        out_specs=(vm, vm),
-        compiler_params=pltpu.CompilerParams(vmem_limit_bytes=32 * 1024 * 1024),
-    )(x, gain, routing)
-
-
-def expert_kernel(rows_ref, wg_ref, wu_ref, wd_ref, out_ref):
-    rows = rows_ref[...]
-    hidden = (silu(dot(rows, wg_ref[...])) * dot(rows, wu_ref[...])).astype(BF16)
-    out_ref[...] = dot(hidden, wd_ref[...]).astype(out_ref.dtype)
-
-
-def expert(rows, wg, wu, wd, dtype, step):
-    n = rows.shape[0]
-    whole = lambda w: pl.BlockSpec(w.shape, lambda i: (0, 0))
-    return pl.pallas_call(
-        expert_kernel,
-        name="expert",
-        grid=(n // step,),
-        out_shape=jax.ShapeDtypeStruct((n, 2048), dtype),
-        in_specs=[pl.BlockSpec((step, 2048), lambda i: (i, 0)), whole(wg), whole(wu), whole(wd)],
-        out_specs=pl.BlockSpec((step, 2048), lambda i: (i, 0)),
-        compiler_params=pltpu.CompilerParams(vmem_limit_bytes=40 * 1024 * 1024),
-        cost_estimate=pl.CostEstimate(flops=6 * n * 2048 * 512, bytes_accessed=15_000_000, transcendentals=0),
-    )(rows, wg, wu, wd)
-
-
-def combine_kernel(back_ref, routing_ref, weight_ref, shared_ref, out_ref):
-    hi, lo = slot_matrix(routing_ref[...], weight_ref[...])
-    for t in range(4):
-        cols = slice(t * 512, (t + 1) * 512)
-        back = back_ref[:, cols]
-        total = dot(hi, back, TN) + dot(lo, back, TN) + shared_ref[:, cols]
-        out_ref[:, cols] = total.astype(BF16)
-
-
-def combine(back, routing, weight, shared):
-    vm = pl.BlockSpec(memory_space=pltpu.VMEM)
-    return pl.pallas_call(
-        combine_kernel,
-        name="combine",
+        moe_kernel,
+        name="moe",
         out_shape=jax.ShapeDtypeStruct((N_TOK, 2048), BF16),
-        in_specs=[vm] * 4,
+        in_specs=[vm, vm, vm] + [hbm] * 6,
         out_specs=vm,
-        compiler_params=pltpu.CompilerParams(vmem_limit_bytes=32 * 1024 * 1024),
-    )(back, routing, weight, shared)
+        scratch_shapes=list(MOE_SCRATCH.values()),
+        compiler_params=pltpu.CompilerParams(
+            collective_id=1, has_side_effects=True, vmem_limit_bytes=60 * 1024 * 1024
+        ),
+        cost_estimate=pl.CostEstimate(flops=9_000_000_000, bytes_accessed=16_000_000, transcendentals=0),
+    )(x, gain.reshape(1, -1), meta, wg, wu, wd, sg, su, sd)
 
 
 def local(
@@ -459,16 +666,11 @@
     moe_input, norm_gain, routing, route_weight,
     expert_gate, expert_up, expert_down, shared_gate, shared_up, shared_down,
 ):
-    slots, normed = dispatch(moe_input, norm_gain.reshape(1, -1), routing)
-    exchange = lambda r: lax.all_to_all(
-        r.reshape(N_EXP, CAP, 2048), EP_TP, split_axis=0, concat_axis=0, tiled=True
-    ).reshape(SLOTS, 2048)
-    received = exchange(slots)
     mixer_out = mixer_half(query_rows, key_rows, value_rows, gate_rows, log_decay, out_proj)
-    served = expert(received, expert_gate[0], expert_up[0], expert_down[0], BF16, 256)
-    returned = exchange(served)
-    shared = expert(normed, shared_gate, shared_up, shared_down, F32, 128)
-    moe_out = combine(returned, routing, route_weight, shared)
+    moe_out = moe_half(
+        moe_input, norm_gain, routing, route_weight,
+        expert_gate, expert_up, expert_down, shared_gate, shared_up, shared_down,
+    )
     return (mixer_out, moe_out)
 
 

time: 196 us -> 204 us (1.041)
  Pallas kernels: 118 us -> 197 us
  blocking collectives: 62.4 us -> 0 us
  starting transfers between devices: 6.54 us -> 0 us
    pallas_call x4 -> x1, Pallas kernels: 16.7 us -> 129 us  [moe_half(): pl.pallas_call(moe_kernel, name='moe', out_shape=jax.ShapeDtypeStruct((N_...]
    all_to_all x1 -> x0, blocking collectives: 62.4 us -> none  [local(): lax.all_to_all(r.reshape(N_EXP, CAP, 2048), EP_TP, split_axis=0, concat_a...]
    pallas_call x1, Pallas kernels: 101 us -> 67.6 us  [mixer_half(): pl.pallas_call(mixer_kernel, name='mixer', out_shape=jax.ShapeDtypeStruct...]
    all_to_all x1 -> x0, starting transfers between devices: 6.54 us -> none  [local(): lax.all_to_all(r.reshape(N_EXP, CAP, 2048), EP_TP, split_axis=0, concat_a...]
    unnamed x31 -> x16, local copies, waits for them, and re-layouts: 5.98 us -> 5.33 us
  transfers between devices with their start and end apart: 1 -> 0, of which waited for: 0 -> 0; matrix products, arithmetic and copies ran while one was open for 0% -> 0% of each run, Pallas kernels for 53% -> 0%
where the time goes in v2:
time: 204 us
  Pallas kernels  197 us (97%)
  local copies, waits for them, and re-layouts  5.33 us (3%)
    pallas_call x1, Pallas kernels, moe_half(): pl.pallas_call(moe_kernel, name='moe', out_shape=jax.ShapeDtypeStruct((N_...  129 us
    pallas_call x1, Pallas kernels, mixer_half(): pl.pallas_call(mixer_kernel, name='mixer', out_shape=jax.ShapeDtypeStruct...  67.6 us
    unnamed x16, local copies, waits for them, and re-layouts  5.33 us

profile of v2, /device:TPU:6, one launch (start us, length us, event | category | flops | bytes accessed | tf_op | source)
XLA Modules:
  0.0 203.7 jit_solution(11668098083251626508)
XLA Ops:
  0.6 0.0 copy-start
  0.6 1.2 copy-done
  1.9 0.0 copy-start.1
  1.9 1.2 copy-done.1
  3.1 0.0 copy-start.2
  3.1 0.7 copy-done.2
  3.8 0.0 copy-start.5
  3.8 0.0 copy-start.6
  3.8 67.6 %mixer.1 = bf16[512,2048]{1,0:T(8,128)(2,1)} custom-call(bf16[2048,256]{1,0:T(8,128)(2,1)S(1)} %copy-done, bf16[2048,256]{1,0:T(8,128)(2,1)S(1)} %copy-done.1, bf16[2048,512]{1,0:T(8,128)(2,1)} %v_ref.1, bf16[2048,512]{1,0:T(8,128)(2,1)} %g_ref.1, f32[2,2048]{1,0:T(2,128)S(1)} %copy-done.2, bf16[512,2048]{1,0:T(8,128)(2,1)} %wo_ref.1), custom_call_target="tpu_custom_call" | custom-call | flops 40000000000 | bytes 16000000 | tf_op jit(solution)/shard_map/mixer/pallas_call | solution.py:320
  71.4 0.0 copy-done.5
  71.5 0.0 copy-done.6
  71.5 0.6 pad_maximum_fusion.meta_ref
  72.1 0.0 copy-start.3
  72.1 129.4 %moe.1 = bf16[128,2048]{1,0:T(8,128)(2,1)} custom-call(bf16[128,2048]{1,0:T(8,128)(2,1)} %x_ref.1, f32[1,2048]{1,0:T(1,128)} %bitcast.5, f32[8,128]{1,0:T(8,128)} %pad_maximum_fusion.meta_ref, bf16[1,2048,512]{2,1,0:T(8,128)(2,1)} %wg.1, bf16[1,2048,512]{2,1,0:T(8,128)(2,1)} %wu.1, bf16[1,512,2048]{2,1,0:T(8,128)(2,1)} %wd.1, bf16[2048,512]{1,0:T(8,128)(2,1)} %sg.1, ...), custom_call_target="tpu_custom_call" | custom-call | flops 8999999488 | bytes 16000000 | tf_op jit(solution)/shard_map/moe/pallas_call | solution.py:650
  201.5 0.0 copy-done.3
  201.5 0.0 copy-start.4
  201.5 1.3 copy.20
  202.8 0.0 copy-done.4
  202.9 0.8 copy.21
  (1 shorter events, 0.0 us)
Async XLA Ops:
  0.6 1.2 copy-start
  1.9 1.2 copy-start.1
  3.1 0.7 copy-start.2
  3.8 67.6 %copy-start.5 = (s32[128,4]{0,1:T(4,128)S(1)}, s32[128,4]{0,1:T(4,128)}, u32[]{:S(2)}) copy-start(s32[128,4]{0,1:T(4,128)} %param.24) | copy-start | bytes 6148
  3.8 67.7 %copy-start.6 = (f32[128,4]{0,1:T(4,128)S(1)}, f32[128,4]{0,1:T(4,128)}, u32[]{:S(2)}) copy-start(f32[128,4]{0,1:T(4,128)} %param.25) | copy-start | bytes 6148
  72.1 129.4 %copy-start.3 = (bf16[512,2048]{1,0:T(8,128)(2,1)S(1)}, bf16[512,2048]{1,0:T(8,128)(2,1)}, u32[]{:S(2)}) copy-start(bf16[512,2048]{1,0:T(8,128)(2,1)} %mixer.1) | copy-start | bytes 6291460
  201.5 1.4 copy-start.4

commit v3 on v2

v3 whole, which is shorter than its diff:
```python
import functools

import jax
import jax.numpy as jnp
from jax import lax
from jax.experimental import pallas as pl
from jax.experimental.pallas import tpu as pltpu
from jax.sharding import Mesh
from jax.sharding import PartitionSpec as P

DK = 128
DV = 256
BLOCK = 128
EP = ("ep_0", "ep_1", "ep_2")
EP_TP = ("ep_0", "ep_1", "ep_2", "tp")
EPS = 1e-06
MESH = pl.DeviceIdType.MESH
HI = lax.Precision.HIGHEST
F32 = jnp.float32
BF16 = jnp.bfloat16
SCALE = DK ** (-0.5)

NT = (((1,), (1,)), ((), ()))
TN = (((0,), (0,)), ((), ()))


def dot(a, b, dims=None, precision=None):
    if dims is None:
        dims = (((1,), (0,)), ((), ()))
    return lax.dot_general(a, b, dims, precision=precision, preferred_element_type=F32)


def iota(shape, dim):
    return lax.broadcasted_iota(jnp.int32, shape, dim)


def silu(v):
    half = 0.5 * v
    return half * jnp.tanh(half) + half


N_BLK = 16
HEADS = 2
PAY = DK + 16


def mixer_steps(ctx, q_hbm, k_hbm, v_hbm, g_hbm, ld_ref, wo_ref, out_ref, s):
    z, y, c, x = ctx.z, ctx.y, ctx.c, ctx.x
    start, copy, mod = ctx.start, ctx.copy, ctx.mod
    nb = HEADS * N_BLK

    def rows(first, n):
        return pl.ds(pl.multiple_of(first, 16), n)

    whole = pl.ds(0, 2048)
    direct, half0, half1 = pl.ds(0, 1024), pl.ds(1024, 512), pl.ds(1536, 512)
    r0 = c * 256 + y * 64 + z * 16
    r1 = c * 256 + z * 64 + y * 16
    loads = {}

    def fetch():
        for i, (name, src, dst) in enumerate(
            (("k", k_hbm, s.k), ("v", v_hbm, s.v), ("q", q_hbm, s.q), ("g", g_hbm, s.g), ("w", wo_ref, s.W.at[0]))
        ):
            loads[name] = pltpu.make_async_copy(src, dst, s.in_sem.at[i])
            loads[name].start()

    wx, wd = [], []

    def spread_x():
        for d in (1, 3, 2):
            for h, (r, cols) in enumerate(((r0, half0), (r1, half1))):
                i = (d - 1) * 2 + h
                wx.append(
                    start(wo_ref.at[rows(r, 16), cols], s.W.at[4 - d, rows(r, 16), cols], s.wx_s.at[i], s.wx_r.at[i], tp=d)
                )
        for d in (1, 3, 2):
            r = rows(c * 256, 256)
            wd.append(start(wo_ref.at[r, direct], s.W.at[4 - d, r, direct], s.wd_s.at[d - 1], s.wd_r.at[d - 1], tp=d))

    def decays():
        for h in range(HEADS):
            for j in range(N_BLK):
                s.a[h * N_BLK + j : h * N_BLK + j + 1, :] = ld_ref[h : h + 1, j * BLOCK : (j + 1) * BLOCK]
        upper = (iota((BLOCK, BLOCK), 0) <= iota((BLOCK, BLOCK), 1)).astype(F32)
        cum = dot(s.a[...], upper, precision=HI)
        s.cum[...] = cum
        totb = jnp.broadcast_to(cum[:, BLOCK - 1 : BLOCK], (nb, BLOCK))
        ri, ci = iota((nb, nb), 0), iota((nb, nb), 1)
        same = (ri // N_BLK) == (ci // N_BLK)
        after = dot((same & (ci > ri)).astype(F32), totb, precision=HI)
        ahead = dot((same & (ci < ri)).astype(F32), totb, precision=HI)
        s.e[...] = jnp.exp(after + totb - cum) * SCALE
        s.fac[...] = jnp.exp(ahead)
        full = jnp.exp(after + totb)
        s.run[...] = jnp.zeros_like(s.run)
        for h in range(HEADS):
            f = full[h * N_BLK : h * N_BLK + 1, :]
            s.tot_f[h] = jnp.concatenate([f, f], axis=1)

    def col(row):
        return jnp.broadcast_to(row, (BLOCK, BLOCK)).T

    def block(j):
        return pl.ds(pl.multiple_of(j * BLOCK, BLOCK), BLOCK)

    def summary():
        loads["k"].wait()
        loads["v"].wait()

        def body(j, _):
            sl = block(j)
            for h in range(HEADS):
                kb = s.k[sl, h * DK : (h + 1) * DK].astype(F32)
                vb = s.v[sl, h * DV : (h + 1) * DV]
                kd = (kb * col(s.e[pl.ds(h * N_BLK + j, 1), :])).astype(BF16)
                s.run[h] += dot(kd, vb, TN)
            return 0

        lax.fori_loop(0, N_BLK, body, 0)
        for h in range(HEADS):
            s.tot_S[h] = s.run[h]
            s.bef_S[h] = jnp.zeros((DK, DV), F32)
            s.bef_f[h] = jnp.ones((1, DV), F32)
        s.run[...] = jnp.zeros_like(s.run)
        loads["q"].wait()

    states = {"ep_2": (s.got_c, 0), "ep_1": (s.got_y, 1), "ep_0": (s.got_z, 4)}
    flying = {}

    def publish(axis):
        got, base = states[axis]
        for h in range(HEADS):
            s.pay[base and 1 + base // 4, h, 0:DK, :] = s.tot_S[h].astype(BF16)
            f = s.tot_f[h]
            f1 = f.astype(BF16)
            f2 = (f - f1.astype(F32)).astype(BF16)
            row = iota((16, DV), 0)
            top = jnp.where(row == 0, f1.astype(F32), jnp.where(row == 1, f2.astype(F32), 0.0))
            s.pay[base and 1 + base // 4, h, DK:PAY, :] = top.astype(BF16)
        flying[axis] = [
            start(
                s.pay.at[base and 1 + base // 4], got.at[d - 1],
                s.pre_s.at[base + d - 1], s.pre_r.at[base + d - 1], **{axis: d}
            )
            for d in range(1, ctx.size[axis])
        ]

    def absorb(axis):
        got, _ = states[axis]
        n, at = ctx.size[axis], ctx.place[axis]
        for cp in flying[axis]:
            cp.wait_recv()
        for h in range(HEADS):
            sub_f = jnp.ones((1, DV), F32)
            sub_S = jnp.zeros((DK, DV), F32)
            in_f, in_S = sub_f, sub_S
            for kk in range(n):
                own = at == kk
                slot = jnp.maximum(lax.rem(at - kk + n, n) - 1, 0)
                piece = got[slot, h].astype(F32)
                pf = piece[DK : DK + 1, :] + piece[DK + 1 : DK + 2, :]
                pf = jnp.where(own, s.tot_f[h], pf)
                ps = jnp.where(own, s.tot_S[h], piece[0:DK, :])
                if kk:
                    in_f = jnp.where(own, sub_f, in_f)
                    in_S = jnp.where(own, sub_S, in_S)
                sub_S = pf * sub_S + ps
                sub_f = sub_f * pf
            s.bef_S[h] = s.bef_f[h] * in_S + s.bef_S[h]
            s.bef_f[h] = s.bef_f[h] * in_f
            s.tot_S[h] = sub_S
            s.tot_f[h] = sub_f

    def inside(lo, hi):
        causal = iota((BLOCK, BLOCK), 0) >= iota((BLOCK, BLOCK), 1)

        def body(j, _):
            sl = block(j)
            for h in range(HEADS):
                qb = s.q[sl, h * DK : (h + 1) * DK]
                kb = s.k[sl, h * DK : (h + 1) * DK]
                vb = s.v[sl, h * DV : (h + 1) * DV]
                crow = s.cum[pl.ds(h * N_BLK + j, 1), :]
                ccol = col(crow)
                gap = ccol - jnp.broadcast_to(crow, (BLOCK, BLOCK))
                dec = jnp.exp(jnp.where(causal, gap, -1e30)) * SCALE
                w = (dot(qb, kb, NT) * dec).astype(BF16)
                s.inner[sl, h * DV : (h + 1) * DV] = dot(w, vb)
                last = crow[:, BLOCK - 1 : BLOCK]
                kd = (kb.astype(F32) * (jnp.exp(last - ccol) * SCALE)).astype(BF16)
                s.prev[h * N_BLK + j] = s.run[h].astype(BF16)
                s.run[h] = s.run[h] * jnp.exp(last) + dot(kd, vb, TN)
            return 0

        lax.fori_loop(lo, hi, body, 0)

    def near(axis, d, r, n, cols, ss, rs):
        ref = s.W.at[1:4, rows(r, n), cols]
        return copy(ref, ref, ss, rs, **{axis: d})

    def ring(n, plan, ss, rs, out, into):
        for d in (1, 3, 2):
            for h, (axis, mine, theirs, cols) in enumerate(plan):
                i = (d - 1) * 2 + h
                cp = near(axis, d, mine, n, cols, ss.at[i], rs.at[i])
                cp.start()
                out.append(cp)
                into.append(near(axis, d, theirs(d), n, cols, ss.at[i], rs.at[i]))

    first, first_in, second, second_in, third = [], [], [], [], []

    def spread_1():
        for cp in wx:
            cp.wait_recv()
        ring(
            16,
            (
                ("ep_0", r0, lambda d: c * 256 + y * 64 + mod(z + 4 - d) * 16, half0),
                ("ep_1", r1, lambda d: c * 256 + z * 64 + mod(y + 4 - d) * 16, half1),
            ),
            s.w1_s, s.w1_r, first, first_in,
        )

    def spread_2():
        for cp in first_in:
            cp.wait_recv()
        ring(
            64,
            (
                ("ep_1", c * 256 + y * 64, lambda d: c * 256 + mod(y + 4 - d) * 64, half0),
                ("ep_0", c * 256 + z * 64, lambda d: c * 256 + mod(z + 4 - d) * 64, half1),
            ),
            s.w2_s, s.w2_r, second, second_in,
        )

    def spread_3():
        for cp in second_in + wd:
            cp.wait_recv()
        cp = near("ep_2", 1, c * 256, 256, whole, s.w3_s, s.w3_r)
        cp.start()
        third.extend([cp, near("ep_2", 1, (1 - c) * 256, 256, whole, s.w3_s, s.w3_r)])

    sends = {}

    def outer(d):
        p = mod(x + d)

        def body(i, _):
            j = p * 4 + i
            sl = block(j)
            for h in range(HEADS):
                qb = s.q[sl, h * DK : (h + 1) * DK]
                crow = s.cum[pl.ds(h * N_BLK + j, 1), :]
                grow = jnp.exp(col(crow))
                grow = jnp.concatenate([grow, grow], axis=1)
                fac = s.fac[pl.ds(h * N_BLK + j, 1), :]
                fac = jnp.concatenate([fac, fac], axis=1)
                state = s.prev[h * N_BLK + j].astype(F32) + s.bef_S[h] * fac
                cross = dot(qb, state.astype(BF16))
                raw = s.inner[sl, h * DV : (h + 1) * DV] + cross * grow
                dev = raw - jnp.mean(raw, axis=-1, keepdims=True)
                n = dev * lax.rsqrt(jnp.mean(dev * dev, axis=-1, keepdims=True) + EPS)
                gate = silu(s.g[sl, h * DV : (h + 1) * DV].astype(F32))
                s.g[sl, h * DV : (h + 1) * DV] = (gate * n).astype(BF16)
            return 0

        lax.fori_loop(0, 4, body, 0)
        if d:
            sends[d] = start(
                s.g.at[rows(p * 512, 512), :], s.R.at[3 - d], s.ret_s.at[d - 1], s.ret_r.at[d - 1], tp=d
            )

    def ready():
        loads["w"].wait()
        for cp in sends.values():
            cp.wait_recv()
        third[1].wait_recv()

    def project(lo, hi):
        def body(t, _):
            cols = pl.ds(pl.multiple_of(t * 512, 512), 512)
            acc = dot(s.g[rows(x * 512, 512), :], s.W[0, :, cols])
            for g in (1, 2, 3):
                acc += dot(s.R[g - 1], s.W[g, :, cols])
            out_ref[:, cols] = acc.astype(BF16)
            return 0

        lax.fori_loop(lo, hi, body, 0)

    def finish():
        for cp in wx + wd + first + second + third[:1] + list(sends.values()) + sum(flying.values(), []):
            cp.wait_send()

    def gate_in():
        loads["g"].wait()

    return dict(
        fetch=fetch, spread_x=spread_x, decays=decays, summary=summary, publish=publish, absorb=absorb, inside=inside,
        spread_1=spread_1, spread_2=spread_2, spread_3=spread_3, outer=outer, ready=ready, project=project,
        finish=finish, gate_in=gate_in,
    )


N_TOK = 128
TOP = 4
CAP = 8
N_EP = 32
ROWS = N_EP * CAP
HALF = 1024


def moe_steps(ctx, x_ref, gain_ref, meta_ref, wg_hbm, wu_hbm, wd_hbm, sg_hbm, su_hbm, sd_hbm, out_ref, s):
    z, y, c, x = ctx.z, ctx.y, ctx.c, ctx.x
    start, mod = ctx.start, ctx.mod

    def fetch(first, *sources):
        for i, (src, dst) in enumerate(zip(sources, (s.wg, s.wu, s.wd))):
            cp = pltpu.make_async_copy(src, dst, s.load.at[first + i])
            cp.start()
            loads.append(cp)

    loads = []
    fetch(0, sg_hbm, su_hbm, sd_hbm)

    v = x_ref[...].astype(F32)
    s.X[0] = (v * lax.rsqrt(jnp.mean(v * v, axis=-1, keepdims=True) + EPS) * gain_ref[...]).astype(BF16)
    s.meta[0] = meta_ref[...]
    gathers = {}
    sends = []
    for d in (1, 3, 2):
        a = start(s.meta.at[0], s.meta.at[4 - d], s.gm_s.at[d - 1], s.gm_r.at[d - 1], tp=d)
        b = start(s.X.at[0], s.X.at[4 - d], s.gx_s.at[d - 1], s.gx_r.at[d - 1], tp=d)
        gathers[4 - d] = (a, b)
        sends += [a, b]

    def build(gg):
        if gg:
            for cp in gathers[gg]:
                cp.wait_recv()
        rt = s.meta[gg, 0:TOP, :]
        wt = s.meta[gg, TOP : 2 * TOP, :]
        ident = (iota((N_EP, N_TOK), 0) * 4 + x).astype(F32)
        named = jnp.zeros((N_EP, N_TOK), F32)
        weight = jnp.zeros((N_EP, N_TOK), F32)
        for kk in range(TOP):
            hit = rt[kk : kk + 1, :] == ident
            named = named + jnp.where(hit, 1.0, 0.0)
            weight = weight + jnp.where(hit, wt[kk : kk + 1, :], 0.0)
        named = named.astype(BF16)
        earlier = (iota((N_TOK, N_TOK), 0) < iota((N_TOK, N_TOK), 1)).astype(F32).astype(BF16)
        rank = dot(named, earlier).astype(BF16)
        slot = iota((ROWS, N_EP), 0)
        spread = (slot // CAP == iota((ROWS, N_EP), 1)).astype(F32).astype(BF16)
        at = (iota((ROWS, N_TOK), 0) % CAP).astype(F32)
        live = (dot(spread, named) > 0.5) & (dot(spread, rank) == at)
        hi = weight.astype(BF16)
        lo = (weight - hi.astype(F32)).astype(BF16)
        s.whi[gg] = jnp.where(live, dot(spread, hi), 0.0).astype(BF16)
        s.wlo[gg] = jnp.where(live, dot(spread, lo), 0.0).astype(BF16)
        place = jnp.where(live, 1.0, 0.0).astype(BF16)
        for h in range(2):
            rows = dot(place, s.X[gg, :, h * HALF : (h + 1) * HALF]).astype(BF16)
            s.D[gg, h] = rows.reshape(4, 4, 2, CAP, HALF)
        s.M[gg, 0, z] = s.D[gg, 0, z]
        for zz in range(4):
            s.M[gg, 1, y, zz] = s.D[gg, 1, zz, y]
        for d in (1, 3, 2):
            zp, yp = mod(z + d), mod(y + d)
            first[gg, 0].append(
                start(s.D.at[gg, 0, zp], s.M.at[gg, 0, z], s.a_s.at[gg, 0, d - 1], s.a_r.at[gg, 0, d - 1], ep_0=d)
            )
            first[gg, 1].append(
                start(s.D.at[gg, 1, :, yp], s.M.at[gg, 1, y], s.a_s.at[gg, 1, d - 1], s.a_r.at[gg, 1, d - 1], ep_1=d)
            )

    first = {(gg, h): [] for gg in range(4) for h in range(2)}
    second = {(gg, h): [] for gg in range(4) for h in range(2)}
    third = {(gg, h): [] for gg in range(4) for h in range(2)}
    fourth = {(gg, h): [] for gg in range(4) for h in range(2)}
    hops = [(1, 0), (3, 0), (1, 1), (3, 1), (2, 0), (2, 1), (0, 1)]

    def relay(gg):
        for h in range(2):
            for cp in first[gg, h]:
                cp.wait_recv()
            for i, (d, e) in enumerate(hops):
                zp, yp, cp_ = mod(z + d), mod(y + d), lax.rem(c + e, 2)
                if h == 0:
                    src, dst = s.M.at[gg, 0, :, yp, cp_], s.V.at[gg, 0, :, y, c]
                    to = {"ep_1": d, "ep_2": e}
                else:
                    src, dst = s.M.at[gg, 1, :, zp, cp_], s.V.at[gg, 1, z, :, c]
                    to = {"ep_0": d, "ep_2": e}
                second[gg, h].append(start(src, dst, s.b_s.at[gg, h, i], s.b_r.at[gg, h, i], **to))
            for k in range(4):
                if h == 0:
                    s.V[gg, 0, k, y, c] = s.M[gg, 0, k, y, c]
                else:
                    s.V[gg, 1, z, k, c] = s.M[gg, 1, k, z, c]

    def expert(gg):
        for h in range(2):
            for cp in second[gg, h]:
                cp.wait_recv()
        a = s.V[gg, 0].reshape(ROWS, HALF)
        b = s.V[gg, 1].reshape(ROWS, HALF)
        gate = dot(a, s.wg[0:HALF]) + dot(b, s.wg[HALF:])
        up = dot(a, s.wu[0:HALF]) + dot(b, s.wu[HALF:])
        hidden = (silu(gate) * up).astype(BF16)
        for h in range(2):
            rows = dot(hidden, s.wd[:, h * HALF : (h + 1) * HALF]).astype(BF16)
            s.V[gg, h] = rows.reshape(4, 4, 2, CAP, HALF)

    def give_back(gg):
        for h in range(2):
            for i, (d, e) in enumerate(hops):
                zp, yp, cp_ = mod(z + d), mod(y + d), lax.rem(c + e, 2)
                if h == 0:
                    src, dst = s.V.at[gg, 0, :, yp, cp_], s.N.at[gg, 0, :, y, c]
                    to = {"ep_1": d, "ep_2": e}
                else:
                    src, dst = s.V.at[gg, 1, zp, :, cp_], s.N.at[gg, 1, :, z, c]
                    to = {"ep_0": d, "ep_2": e}
                third[gg, h].append(start(src, dst, s.c_s.at[gg, h, i], s.c_r.at[gg, h, i], **to))
            for k in range(4):
                if h == 0:
                    s.N[gg, 0, k, y, c] = s.V[gg, 0, k, y, c]
                else:
                    s.N[gg, 1, k, z, c] = s.V[gg, 1, z, k, c]

    def relay_back(gg):
        for h in range(2):
            for cp in third[gg, h]:
                cp.wait_recv()
            for d in (1, 3, 2):
                zp, yp = mod(z + d), mod(y + d)
                if h == 0:
                    cp = start(s.N.at[gg, 0, zp], s.B.at[gg, 0, z], s.d_s.at[gg, 0, d - 1], s.d_r.at[gg, 0, d - 1], ep_0=d)
                else:
                    cp = start(s.N.at[gg, 1, yp], s.B.at[gg, 1, :, y], s.d_s.at[gg, 1, d - 1], s.d_r.at[gg, 1, d - 1], ep_1=d)
                fourth[gg, h].append(cp)
            if h == 0:
                s.B[gg, 0, z] = s.N[gg, 0, z]
            else:
                for zz in range(4):
                    s.B[gg, 1, zz, y] = s.N[gg, 1, y, zz]

    reduces = {}

    def fold(gg):
        for h in range(2):
            cols = slice(h * HALF, (h + 1) * HALF)
            for cp in fourth[gg, h]:
                cp.wait_recv()
            back = s.B[gg, h].reshape(ROWS, HALF)
            part = dot(s.whi[gg], back, TN) + dot(s.wlo[gg], back, TN)
            if gg == 0:
                s.acc[:, cols] = s.acc[:, cols] + part
            else:
                s.P[gg - 1, h] = part.astype(BF16)
                reduces[gg, h] = start(
                    s.P.at[gg - 1, h], s.G.at[gg - 1, h], s.e_s.at[gg - 1, h], s.e_r.at[gg - 1, h], tp=gg
                )

    def shared():
        for cp in loads[:3]:
            cp.wait()
        rows = s.X[0]
        hidden = (silu(dot(rows, s.wg[...])) * dot(rows, s.wu[...])).astype(BF16)
        for h in range(2):
            cols = slice(h * HALF, (h + 1) * HALF)
            s.acc[:, cols] = dot(hidden, s.wd[:, cols])
        fetch(3, wg_hbm.at[0], wu_hbm.at[0], wd_hbm.at[0])

    def finish():
        for h in range(2):
            cols = slice(h * HALF, (h + 1) * HALF)
            total = s.acc[:, cols]
            for gg in (1, 2, 3):
                reduces[gg, h].wait_recv()
                total = total + s.G[gg - 1, h].astype(F32)
            out_ref[:, cols] = total.astype(BF16)
        for group in (first, second, third, fourth):
            for cps in group.values():
                for cp in cps:
                    cp.wait_send()
        for cp in list(reduces.values()) + sends:
            cp.wait_send()

    def weights():
        for cp in loads[3:]:
            cp.wait()

    return dict(
        build=build, relay=relay, expert=expert, give_back=give_back, relay_back=relay_back,
        fold=fold, shared=shared, finish=finish, weights=weights,
    )


class Names:
    pass


class Ctx:
    def __init__(self):
        self.z = lax.axis_index("ep_0")
        self.y = lax.axis_index("ep_1")
        self.c = lax.axis_index("ep_2")
        self.x = lax.axis_index("tp")
        self.place = {"ep_0": self.z, "ep_1": self.y, "ep_2": self.c, "tp": self.x}
        self.size = {"ep_0": 4, "ep_1": 4, "ep_2": 2, "tp": 4}

    def mod(self, v):
        return lax.rem(v, 4)

    def peer(self, **offsets):
        return {a: lax.rem(self.place[a] + d, self.size[a]) for a, d in offsets.items() if d}

    def copy(self, src, dst, send, recv, **offsets):
        return pltpu.make_async_remote_copy(
            src_ref=src, dst_ref=dst, send_sem=send, recv_sem=recv,
            device_id=self.peer(**offsets), device_id_type=MESH,
        )

    def start(self, src, dst, send, recv, **offsets):
        cp = self.copy(src, dst, send, recv, **offsets)
        cp.start()
        return cp


def greet(ctx):
    peers = [dict(tp=d) for d in (1, 2, 3)]
    peers += [dict(ep_0=d, ep_2=e) for d in (1, 2, 3) for e in (0, 1)]
    peers += [dict(ep_1=d, ep_2=e) for d in (1, 2, 3) for e in (0, 1)]
    peers += [dict(ep_2=1)]
    barrier = pltpu.get_barrier_semaphore()
    for p in peers:
        pl.semaphore_signal(barrier, inc=1, device_id=ctx.peer(**p), device_id_type=MESH)
    pl.semaphore_wait(barrier, len(peers))


DMA = pltpu.SemaphoreType.DMA
BLK = (4, 4, 2, CAP, HALF)
SCRATCH = dict(
    wg=pltpu.VMEM((2048, 512), BF16), wu=pltpu.VMEM((2048, 512), BF16), wd=pltpu.VMEM((512, 2048), BF16),
    X=pltpu.VMEM((4, N_TOK, 2048), BF16), meta=pltpu.VMEM((4, 8, N_TOK), F32),
    whi=pltpu.VMEM((4, ROWS, N_TOK), BF16), wlo=pltpu.VMEM((4, ROWS, N_TOK), BF16),
    D=pltpu.VMEM((4, 2) + BLK, BF16), M=pltpu.VMEM((4, 2) + BLK, BF16), V=pltpu.VMEM((4, 2) + BLK, BF16),
    N=pltpu.VMEM((4, 2) + BLK, BF16), B=pltpu.VMEM((4, 2) + BLK, BF16),
    acc=pltpu.VMEM((N_TOK, 2048), F32),
    P=pltpu.VMEM((3, 2, N_TOK, HALF), BF16), G=pltpu.VMEM((3, 2, N_TOK, HALF), BF16),
    load=DMA((6,)),
    gm_s=DMA((3,)), gm_r=DMA((3,)), gx_s=DMA((3,)), gx_r=DMA((3,)),
    a_s=DMA((4, 2, 3)), a_r=DMA((4, 2, 3)), b_s=DMA((4, 2, 7)), b_r=DMA((4, 2, 7)),
    c_s=DMA((4, 2, 7)), c_r=DMA((4, 2, 7)), d_s=DMA((4, 2, 3)), d_r=DMA((4, 2, 3)),
    e_s=DMA((3, 2)), e_r=DMA((3, 2)),
    q=pltpu.VMEM((2048, 256), BF16), k=pltpu.VMEM((2048, 256), BF16),
    v=pltpu.VMEM((2048, 512), BF16), g=pltpu.VMEM((2048, 512), BF16),
    W=pltpu.VMEM((4, 512, 2048), BF16), R=pltpu.VMEM((3, 512, 512), BF16),
    inner=pltpu.VMEM((2048, 512), F32), prev=pltpu.VMEM((32, DK, DV), BF16),
    a=pltpu.VMEM((32, BLOCK), F32), cum=pltpu.VMEM((32, BLOCK), F32), e=pltpu.VMEM((32, BLOCK), F32),
    fac=pltpu.VMEM((32, BLOCK), F32), run=pltpu.VMEM((2, DK, DV), F32),
    tot_S=pltpu.VMEM((2, DK, DV), F32), tot_f=pltpu.VMEM((2, 1, DV), F32),
    bef_S=pltpu.VMEM((2, DK, DV), F32), bef_f=pltpu.VMEM((2, 1, DV), F32),
    pay=pltpu.VMEM((3, 2, PAY, DV), BF16), got_c=pltpu.VMEM((1, 2, PAY, DV), BF16),
    got_y=pltpu.VMEM((3, 2, PAY, DV), BF16), got_z=pltpu.VMEM((3, 2, PAY, DV), BF16),
    in_sem=DMA((5,)), wx_s=DMA((6,)), wx_r=DMA((6,)), wd_s=DMA((3,)), wd_r=DMA((3,)),
    w1_s=DMA((6,)), w1_r=DMA((6,)), w2_s=DMA((6,)), w2_r=DMA((6,)), w3_s=DMA, w3_r=DMA,
    pre_s=DMA((7,)), pre_r=DMA((7,)), ret_s=DMA((3,)), ret_r=DMA((3,)),
)


def layer_kernel(
    q, k, v, g, ld, wo, x_ref, gain_ref, meta_ref, wg, wu, wd, sg, su, sd, mix_ref, moe_ref, *scratch
):
    ctx = Ctx()
    s = Names()
    for name, ref in zip(SCRATCH, scratch):
        setattr(s, name, ref)
    greet(ctx)
    a = Names()
    m = Names()
    a.__dict__.update(moe_steps(ctx, x_ref, gain_ref, meta_ref, wg, wu, wd, sg, su, sd, moe_ref, s))
    m.__dict__.update(mixer_steps(ctx, q, k, v, g, ld, wo, mix_ref, s))
    m.fetch()
    a.build(0)
    m.spread_x()
    m.decays()
    m.summary()
    m.publish("ep_2")
    a.shared()
    m.inside(0, 2)
    m.absorb("ep_2")
    m.publish("ep_1")
    a.relay(0)
    a.build(1)
    a.build(3)
    m.spread_1()
    m.inside(2, 5)
    m.absorb("ep_1")
    m.publish("ep_0")
    a.relay(1)
    a.relay(3)
    a.weights()
    a.expert(0)
    m.inside(5, 8)
    a.build(2)
    a.expert(1)
    a.give_back(1)
    m.inside(8, 12)
    m.spread_2()
    a.expert(3)
    a.give_back(3)
    a.relay(2)
    m.inside(12, 16)
    m.absorb("ep_0")
    m.gate_in()
    a.relay_back(1)
    m.outer(1)
    a.expert(2)
    a.give_back(2)
    m.outer(3)
    a.relay_back(3)
    a.give_back(0)
    m.outer(2)
    a.fold(1)
    m.outer(0)
    m.spread_3()
    a.relay_back(2)
    a.fold(3)
    a.relay_back(0)
    a.fold(2)
    m.ready()
    m.project(0, 4)
    a.fold(0)
    a.finish()
    m.finish()


def local(
    query_rows, key_rows, value_rows, gate_rows, log_decay, out_proj,
    moe_input, norm_gain, routing, route_weight,
    expert_gate, expert_up, expert_down, shared_gate, shared_up, shared_down,
):
    meta = jnp.concatenate([routing.T.astype(F32), route_weight.T], axis=0)
    vm = pl.BlockSpec(memory_space=pltpu.VMEM)
    hbm = pl.BlockSpec(memory_space=pl.ANY)
    return pl.pallas_call(
        layer_kernel,
        name="layer",
        out_shape=(jax.ShapeDtypeStruct((512, 2048), BF16), jax.ShapeDtypeStruct((N_TOK, 2048), BF16)),
        in_specs=[hbm] * 4 + [vm, hbm] + [vm] * 3 + [hbm] * 6,
        out_specs=(vm, vm),
        scratch_shapes=list(SCRATCH.values()),
        compiler_params=pltpu.CompilerParams(
            collective_id=0, has_side_effects=True, vmem_limit_bytes=67043328
        ),
    )(
        query_rows, key_rows, value_rows, gate_rows, log_decay, out_proj,
        moe_input, norm_gain.reshape(1, -1), meta,
        expert_gate, expert_up, expert_down, shared_gate, shared_up, shared_down,
    )


def solution(mesh):
    split = Mesh(mesh.devices.reshape(4, 4, 2, mesh.shape["tp"]), ("ep_0", "ep_1", "ep_2", "tp"))
    return jax.shard_map(
        local,
        mesh=split,
        in_specs=(
            P(EP, "tp"),
            P(EP, "tp"),
            P(EP, "tp"),
            P(EP, "tp"),
            P("tp", EP),
            P("tp", None),
            P(EP_TP, None),
            P(),
            P(EP_TP, None),
            P(EP_TP, None),
            P(EP_TP, None, None),
            P(EP_TP, None, None),
            P(EP_TP, None, None),
            P(),
            P(),
            P(),
        ),
        out_specs=(P(EP_TP, None), P(EP_TP, None)),
        check_vma=False,
    )
```

time: 204 us -> 157 us (0.77); the launches traced: 204 us -> 155 us
  Pallas kernels: 197 us -> 148 us
    pallas_call x2 -> x1, Pallas kernels: 197 us -> 148 us  [local(): pl.pallas_call(layer_kernel, name='layer', out_shape=(jax.ShapeDtypeStruc...]
    unnamed x16 -> x4, local copies, waits for them, and re-layouts: 5.33 us -> 4.01 us
where the time goes in v3:
time: 157 us; the launch traced here: 155 us
  Pallas kernels  148 us (94%)
  local copies, waits for them, and re-layouts  4.01 us (3%)
  other arithmetic  1.96 us (1%)
    pallas_call x1, Pallas kernels, local(): pl.pallas_call(layer_kernel, name='layer', out_shape=(jax.ShapeDtypeStruc...  148 us
    unnamed x4, local copies, waits for them, and re-layouts  4.01 us

profile of v3, /device:TPU:6, one launch (start us, length us, event | category | flops | bytes accessed | tf_op | source)
XLA Modules:
  0.0 154.5 jit_solution(763249756666384121)
XLA Ops:
  0.6 0.7 convert_bitcast_fusion
  1.3 1.3 pad_maximum_fusion.meta_ref
  2.6 147.9 %layer.1 = (bf16[512,2048]{1,0:T(8,128)(2,1)}, bf16[128,2048]{1,0:T(8,128)(2,1)}) custom-call(bf16[2048,256]{1,0:T(8,128)(2,1)} %q.1, bf16[2048,256]{1,0:T(8,128)(2,1)} %k.1, bf16[2048,512]{1,0:T(8,128)(2,1)} %v.1, bf16[2048,512]{1,0:T(8,128)(2,1)} %g.1, f32[2,2048]{1,0:T(2,128)} %ld.1, bf16[512,2048]{1,0:T(8,128)(2,1)} %wo.1, bf16[128,2048]{1,0:T(8,128)(2,1)} %x_ref.1, ...), custom_call_target="tpu_custom_call" | custom-call | tf_op jit(solution)/shard_map/layer/pallas_call | solution.py:649
  150.5 0.0 copy-start
  150.5 3.2 %copy.20 = bf16[512,2048]{1,0:T(8,128)(2,1)} copy(bf16[512,2048]{1,0:T(8,128)(2,1)} %get-tuple-element.4) | data formatting | bytes 4194304
  153.7 0.0 copy-done
  153.7 0.8 copy.21
Async XLA Ops:
  150.5 3.2 %copy-start = (bf16[128,2048]{1,0:T(8,128)(2,1)S(1)}, bf16[128,2048]{1,0:T(8,128)(2,1)}, u32[]{:S(2)}) copy-start(bf16[128,2048]{1,0:T(8,128)(2,1)} %get-tuple-element.5) | copy-start | bytes 1572868

commit v4 on v3

--- a/solution.py
+++ b/solution.py
@@ -53,7 +53,7 @@
         return pl.ds(pl.multiple_of(first, 16), n)
 
     whole = pl.ds(0, 2048)
-    direct, half0, half1 = pl.ds(0, 1024), pl.ds(1024, 512), pl.ds(1536, 512)
+    direct, half0, half1 = pl.ds(0, 1536), pl.ds(1536, 256), pl.ds(1792, 256)
     r0 = c * 256 + y * 64 + z * 16
     r1 = c * 256 + z * 64 + y * 16
     loads = {}
@@ -74,6 +74,8 @@
                 wx.append(
                     start(wo_ref.at[rows(r, 16), cols], s.W.at[4 - d, rows(r, 16), cols], s.wx_s.at[i], s.wx_r.at[i], tp=d)
                 )
+
+    def spread_d():
         for d in (1, 3, 2):
             r = rows(c * 256, 256)
             wd.append(start(wo_ref.at[r, direct], s.W.at[4 - d, r, direct], s.wd_s.at[d - 1], s.wd_r.at[d - 1], tp=d))
@@ -108,69 +110,91 @@
         loads["k"].wait()
         loads["v"].wait()
 
-        def body(j, _):
-            sl = block(j)
+        def body(b, _):
+            sl = pl.ds(pl.multiple_of(b * 512, 512), 512)
             for h in range(HEADS):
-                kb = s.k[sl, h * DK : (h + 1) * DK].astype(F32)
-                vb = s.v[sl, h * DV : (h + 1) * DV]
-                kd = (kb * col(s.e[pl.ds(h * N_BLK + j, 1), :])).astype(BF16)
-                s.run[h] += dot(kd, vb, TN)
+                scale = jnp.concatenate([col(s.e[pl.ds(h * N_BLK + b * 4 + i, 1), :]) for i in range(4)], axis=0)
+                kd = (s.k[sl, h * DK : (h + 1) * DK].astype(F32) * scale).astype(BF16)
+                s.run[h] += dot(kd, s.v[sl, h * DV : (h + 1) * DV], TN)
             return 0
 
-        lax.fori_loop(0, N_BLK, body, 0)
+        lax.fori_loop(0, 4, body, 0)
         for h in range(HEADS):
             s.tot_S[h] = s.run[h]
-            s.bef_S[h] = jnp.zeros((DK, DV), F32)
-            s.bef_f[h] = jnp.ones((1, DV), F32)
         s.run[...] = jnp.zeros_like(s.run)
         loads["q"].wait()
 
     states = {"ep_2": (s.got_c, 0), "ep_1": (s.got_y, 1), "ep_0": (s.got_z, 4)}
     flying = {}
 
+    def payload(S, f):
+        f1 = f.astype(BF16)
+        f2 = (f - f1.astype(F32)).astype(BF16)
+        row = iota((16, DV), 0)
+        top = jnp.where(row == 0, f1.astype(F32), jnp.where(row == 1, f2.astype(F32), 0.0))
+        return S.astype(BF16), top.astype(BF16)
+
     def publish(axis):
         got, base = states[axis]
-        for h in range(HEADS):
-            s.pay[base and 1 + base // 4, h, 0:DK, :] = s.tot_S[h].astype(BF16)
-            f = s.tot_f[h]
-            f1 = f.astype(BF16)
-            f2 = (f - f1.astype(F32)).astype(BF16)
-            row = iota((16, DV), 0)
-            top = jnp.where(row == 0, f1.astype(F32), jnp.where(row == 1, f2.astype(F32), 0.0))
-            s.pay[base and 1 + base // 4, h, DK:PAY, :] = top.astype(BF16)
+        if axis == "ep_2":
+            src = s.pay_c
+            for h in range(HEADS):
+                src[h, 0:DK, :], src[h, DK:PAY, :] = payload(s.tot_S[h], s.tot_f[h])
+        else:
+            src = s.pay.at[base // 4]
+            src[0:DK, :], src[DK:PAY, :] = payload(s.tot_S[c], s.tot_f[c])
         flying[axis] = [
-            start(
-                s.pay.at[base and 1 + base // 4], got.at[d - 1],
-                s.pre_s.at[base + d - 1], s.pre_r.at[base + d - 1], **{axis: d}
-            )
+            start(src, got.at[d - 1], s.pre_s.at[base + d - 1], s.pre_r.at[base + d - 1], **{axis: d})
             for d in range(1, ctx.size[axis])
         ]
 
+    def scan_over(axis, pieces, own_S, own_f):
+        n, at = ctx.size[axis], ctx.place[axis]
+        sub_f = jnp.ones((1, DV), F32)
+        sub_S = jnp.zeros((DK, DV), F32)
+        in_f, in_S = sub_f, sub_S
+        for kk in range(n):
+            own = at == kk
+            slot = jnp.maximum(lax.rem(at - kk + n, n) - 1, 0)
+            piece = pieces(slot).astype(F32)
+            pf = piece[DK : DK + 1, :] + piece[DK + 1 : DK + 2, :]
+            pf = jnp.where(own, own_f, pf)
+            ps = jnp.where(own, own_S, piece[0:DK, :])
+            if kk:
+                in_f = jnp.where(own, sub_f, in_f)
+                in_S = jnp.where(own, sub_S, in_S)
+            sub_S = pf * sub_S + ps
+            sub_f = sub_f * pf
+        return in_f, in_S, sub_f, sub_S
+
     def absorb(axis):
         got, _ = states[axis]
-        n, at = ctx.size[axis], ctx.place[axis]
         for cp in flying[axis]:
             cp.wait_recv()
+        if axis == "ep_2":
+            for h in range(HEADS):
+                s.bef_f[h], s.bef_S[h], s.tot_f[h], s.tot_S[h] = scan_over(
+                    axis, lambda slot: got[slot, h], s.tot_S[h], s.tot_f[h]
+                )
+            return
+        in_f, in_S, all_f, all_S = scan_over(axis, lambda slot: got[slot], s.tot_S[c], s.tot_f[c])
+        if axis == "ep_1":
+            s.chip_f[...] = in_f
+            s.chip_S[...] = in_S
+            s.tot_f[c] = all_f
+            s.tot_S[c] = all_S
+        else:
+            s.chip_S[...] = s.chip_f[...] * in_S + s.chip_S[...]
+
+    def swap():
+        flying["end"] = [start(s.chip_S, s.got_e, s.end_s, s.end_r, ep_2=1)]
+
+    def settle():
+        for cp in flying["end"]:
+            cp.wait_recv()
         for h in range(HEADS):
-            sub_f = jnp.ones((1, DV), F32)
-            sub_S = jnp.zeros((DK, DV), F32)
-            in_f, in_S = sub_f, sub_S
-            for kk in range(n):
-                own = at == kk
-                slot = jnp.maximum(lax.rem(at - kk + n, n) - 1, 0)
-                piece = got[slot, h].astype(F32)
-                pf = piece[DK : DK + 1, :] + piece[DK + 1 : DK + 2, :]
-                pf = jnp.where(own, s.tot_f[h], pf)
-                ps = jnp.where(own, s.tot_S[h], piece[0:DK, :])
-                if kk:
-                    in_f = jnp.where(own, sub_f, in_f)
-                    in_S = jnp.where(own, sub_S, in_S)
-                sub_S = pf * sub_S + ps
-                sub_f = sub_f * pf
-            s.bef_S[h] = s.bef_f[h] * in_S + s.bef_S[h]
-            s.bef_f[h] = s.bef_f[h] * in_f
-            s.tot_S[h] = sub_S
-            s.tot_f[h] = sub_f
+            before = jnp.where(c == h, s.chip_S[...], s.got_e[...])
+            s.bef_S[h] = s.bef_f[h] * before + s.bef_S[h]
 
     def inside(lo, hi):
         causal = iota((BLOCK, BLOCK), 0) >= iota((BLOCK, BLOCK), 1)
@@ -283,7 +307,8 @@
             acc = dot(s.g[rows(x * 512, 512), :], s.W[0, :, cols])
             for g in (1, 2, 3):
                 acc += dot(s.R[g - 1], s.W[g, :, cols])
-            out_ref[:, cols] = acc.astype(BF16)
+            s.mix[:, cols] = acc.astype(BF16)
+            pltpu.make_async_copy(s.mix.at[:, cols], out_ref.at[:, cols], s.out_sem.at[t]).start()
             return 0
 
         lax.fori_loop(lo, hi, body, 0)
@@ -292,13 +317,18 @@
         for cp in wx + wd + first + second + third[:1] + list(sends.values()) + sum(flying.values(), []):
             cp.wait_send()
 
+    def drain():
+        for t in range(4):
+            cols = pl.ds(t * 512, 512)
+            pltpu.make_async_copy(s.mix.at[:, cols], out_ref.at[:, cols], s.out_sem.at[t]).wait()
+
     def gate_in():
         loads["g"].wait()
 
     return dict(
         fetch=fetch, spread_x=spread_x, decays=decays, summary=summary, publish=publish, absorb=absorb, inside=inside,
         spread_1=spread_1, spread_2=spread_2, spread_3=spread_3, outer=outer, ready=ready, project=project,
-        finish=finish, gate_in=gate_in,
+        finish=finish, gate_in=gate_in, drain=drain, swap=swap, settle=settle, spread_d=spread_d,
     )
 
 
@@ -310,7 +340,7 @@
 HALF = 1024
 
 
-def moe_steps(ctx, x_ref, gain_ref, meta_ref, wg_hbm, wu_hbm, wd_hbm, sg_hbm, su_hbm, sd_hbm, out_ref, s):
+def moe_steps(ctx, x_ref, gain_ref, rt_ref, wt_ref, wg_hbm, wu_hbm, wd_hbm, sg_hbm, su_hbm, sd_hbm, out_ref, s):
     z, y, c, x = ctx.z, ctx.y, ctx.c, ctx.x
     start, mod = ctx.start, ctx.mod
 
@@ -323,16 +353,19 @@
     loads = []
     fetch(0, sg_hbm, su_hbm, sd_hbm)
 
-    v = x_ref[...].astype(F32)
-    s.X[0] = (v * lax.rsqrt(jnp.mean(v * v, axis=-1, keepdims=True) + EPS) * gain_ref[...]).astype(BF16)
-    s.meta[0] = meta_ref[...]
     gathers = {}
     sends = []
-    for d in (1, 3, 2):
-        a = start(s.meta.at[0], s.meta.at[4 - d], s.gm_s.at[d - 1], s.gm_r.at[d - 1], tp=d)
-        b = start(s.X.at[0], s.X.at[4 - d], s.gx_s.at[d - 1], s.gx_r.at[d - 1], tp=d)
-        gathers[4 - d] = (a, b)
-        sends += [a, b]
+
+    def rows_out():
+        v = x_ref[...].astype(F32)
+        s.X[0] = (v * lax.rsqrt(jnp.mean(v * v, axis=-1, keepdims=True) + EPS) * gain_ref[...]).astype(BF16)
+        s.meta[0, 0:TOP, :] = rt_ref[...].astype(F32)
+        s.meta[0, TOP : 2 * TOP, :] = wt_ref[...]
+        for d in (1, 3, 2):
+            a = start(s.meta.at[0], s.meta.at[4 - d], s.gm_s.at[d - 1], s.gm_r.at[d - 1], tp=d)
+            b = start(s.X.at[0], s.X.at[4 - d], s.gx_s.at[d - 1], s.gx_r.at[d - 1], tp=d)
+            gathers[4 - d] = (a, b)
+            sends.extend([a, b])
 
     def build(gg):
         if gg:
@@ -480,20 +513,23 @@
             for gg in (1, 2, 3):
                 reduces[gg, h].wait_recv()
                 total = total + s.G[gg - 1, h].astype(F32)
-            out_ref[:, cols] = total.astype(BF16)
+            s.res[:, cols] = total.astype(BF16)
+        out = pltpu.make_async_copy(s.res, out_ref, s.res_sem)
+        out.start()
         for group in (first, second, third, fourth):
             for cps in group.values():
                 for cp in cps:
                     cp.wait_send()
         for cp in list(reduces.values()) + sends:
             cp.wait_send()
+        out.wait()
 
     def weights():
         for cp in loads[3:]:
             cp.wait()
 
     return dict(
-        build=build, relay=relay, expert=expert, give_back=give_back, relay_back=relay_back,
+        rows_out=rows_out, build=build, relay=relay, expert=expert, give_back=give_back, relay_back=relay_back,
         fold=fold, shared=shared, finish=finish, weights=weights,
     )
 
@@ -563,8 +599,11 @@
     fac=pltpu.VMEM((32, BLOCK), F32), run=pltpu.VMEM((2, DK, DV), F32),
     tot_S=pltpu.VMEM((2, DK, DV), F32), tot_f=pltpu.VMEM((2, 1, DV), F32),
     bef_S=pltpu.VMEM((2, DK, DV), F32), bef_f=pltpu.VMEM((2, 1, DV), F32),
-    pay=pltpu.VMEM((3, 2, PAY, DV), BF16), got_c=pltpu.VMEM((1, 2, PAY, DV), BF16),
-    got_y=pltpu.VMEM((3, 2, PAY, DV), BF16), got_z=pltpu.VMEM((3, 2, PAY, DV), BF16),
+    pay_c=pltpu.VMEM((2, PAY, DV), BF16), pay=pltpu.VMEM((2, PAY, DV), BF16), got_c=pltpu.VMEM((1, 2, PAY, DV), BF16),
+    got_y=pltpu.VMEM((3, PAY, DV), BF16), got_z=pltpu.VMEM((3, PAY, DV), BF16),
+    chip_S=pltpu.VMEM((DK, DV), F32), chip_f=pltpu.VMEM((1, DV), F32), got_e=pltpu.VMEM((DK, DV), F32),
+    end_s=DMA, end_r=DMA,
+    mix=pltpu.VMEM((512, 2048), BF16), res=pltpu.VMEM((N_TOK, 2048), BF16), out_sem=DMA((4,)), res_sem=DMA,
     in_sem=DMA((5,)), wx_s=DMA((6,)), wx_r=DMA((6,)), wd_s=DMA((3,)), wd_r=DMA((3,)),
     w1_s=DMA((6,)), w1_r=DMA((6,)), w2_s=DMA((6,)), w2_r=DMA((6,)), w3_s=DMA, w3_r=DMA,
     pre_s=DMA((7,)), pre_r=DMA((7,)), ret_s=DMA((3,)), ret_r=DMA((3,)),
@@ -572,7 +611,7 @@
 
 
 def layer_kernel(
-    q, k, v, g, ld, wo, x_ref, gain_ref, meta_ref, wg, wu, wd, sg, su, sd, mix_ref, moe_ref, *scratch
+    q, k, v, g, ld, wo, x_ref, gain_ref, rt_ref, wt_ref, wg, wu, wd, sg, su, sd, mix_ref, moe_ref, *scratch
 ):
     ctx = Ctx()
     s = Names()
@@ -581,61 +620,66 @@
     greet(ctx)
     a = Names()
     m = Names()
-    a.__dict__.update(moe_steps(ctx, x_ref, gain_ref, meta_ref, wg, wu, wd, sg, su, sd, moe_ref, s))
+    a.__dict__.update(moe_steps(ctx, x_ref, gain_ref, rt_ref, wt_ref, wg, wu, wd, sg, su, sd, moe_ref, s))
     m.__dict__.update(mixer_steps(ctx, q, k, v, g, ld, wo, mix_ref, s))
+    m.spread_x()
     m.fetch()
+    a.rows_out()
     a.build(0)
-    m.spread_x()
+    m.spread_d()
     m.decays()
+    m.spread_1()
     m.summary()
     m.publish("ep_2")
     a.shared()
-    m.inside(0, 2)
+    m.spread_2()
     m.absorb("ep_2")
     m.publish("ep_1")
     a.relay(0)
+    m.inside(0, 4)
     a.build(1)
     a.build(3)
-    m.spread_1()
-    m.inside(2, 5)
     m.absorb("ep_1")
     m.publish("ep_0")
-    a.relay(1)
-    a.relay(3)
+    m.inside(4, 8)
     a.weights()
     a.expert(0)
-    m.inside(5, 8)
+    a.relay(1)
     a.build(2)
+    m.inside(8, 12)
+    a.relay(3)
+    m.absorb("ep_0")
+    m.swap()
+    m.inside(12, 16)
+    m.settle()
+    m.gate_in()
     a.expert(1)
+    a.relay(2)
     a.give_back(1)
-    m.inside(8, 12)
-    m.spread_2()
+    m.outer(1)
+    m.outer(3)
+    m.outer(2)
     a.expert(3)
     a.give_back(3)
-    a.relay(2)
-    m.inside(12, 16)
-    m.absorb("ep_0")
-    m.gate_in()
-    a.relay_back(1)
-    m.outer(1)
+    m.outer(0)
     a.expert(2)
     a.give_back(2)
-    m.outer(3)
+    m.spread_3()
+    a.relay_back(1)
     a.relay_back(3)
     a.give_back(0)
-    m.outer(2)
     a.fold(1)
-    m.outer(0)
-    m.spread_3()
     a.relay_back(2)
     a.fold(3)
+    m.ready()
+    m.project(0, 2)
     a.relay_back(0)
     a.fold(2)
-    m.ready()
-    m.project(0, 4)
+    m.project(2, 4)
     a.fold(0)
     a.finish()
     m.finish()
+    m.drain()
 
 
 def local(
@@ -643,22 +687,21 @@
     moe_input, norm_gain, routing, route_weight,
     expert_gate, expert_up, expert_down, shared_gate, shared_up, shared_down,
 ):
-    meta = jnp.concatenate([routing.T.astype(F32), route_weight.T], axis=0)
     vm = pl.BlockSpec(memory_space=pltpu.VMEM)
     hbm = pl.BlockSpec(memory_space=pl.ANY)
     return pl.pallas_call(
         layer_kernel,
         name="layer",
         out_shape=(jax.ShapeDtypeStruct((512, 2048), BF16), jax.ShapeDtypeStruct((N_TOK, 2048), BF16)),
-        in_specs=[hbm] * 4 + [vm, hbm] + [vm] * 3 + [hbm] * 6,
-        out_specs=(vm, vm),
+        in_specs=[hbm] * 4 + [vm, hbm] + [vm] * 4 + [hbm] * 6,
+        out_specs=(hbm, hbm),
         scratch_shapes=list(SCRATCH.values()),
         compiler_params=pltpu.CompilerParams(
             collective_id=0, has_side_effects=True, vmem_limit_bytes=67043328
         ),
     )(
         query_rows, key_rows, value_rows, gate_rows, log_decay, out_proj,
-        moe_input, norm_gain.reshape(1, -1), meta,
+        moe_input, norm_gain.reshape(1, -1), routing.T, route_weight.T,
         expert_gate, expert_up, expert_down, shared_gate, shared_up, shared_down,
     )
 

time: 157 us -> 129 us (0.82)
  Pallas kernels: 148 us -> 122 us
  other arithmetic: 1.96 us -> 0 us
    pallas_call x1, Pallas kernels: 148 us -> 122 us  [local(): pl.pallas_call(layer_kernel, name='layer', out_shape=(jax.ShapeDtypeStruc...]
where the time goes in v4:
time: 129 us; the launch traced here: 126 us
  Pallas kernels  122 us (95%)
  local copies, waits for them, and re-layouts  4.01 us (3%)
    pallas_call x1, Pallas kernels, local(): pl.pallas_call(layer_kernel, name='layer', out_shape=(jax.ShapeDtypeStruc...  122 us
    unnamed x4, local copies, waits for them, and re-layouts  4.01 us

profile of v4, /device:TPU:6, one launch (start us, length us, event | category | flops | bytes accessed | tf_op | source)
XLA Modules:
  0.0 126.2 jit_solution(7067617364654632183)
XLA Ops:
  0.6 121.5 %layer.1 = (bf16[512,2048]{1,0:T(8,128)(2,1)}, bf16[128,2048]{1,0:T(8,128)(2,1)}) custom-call(bf16[2048,256]{1,0:T(8,128)(2,1)} %q.1, bf16[2048,256]{1,0:T(8,128)(2,1)} %k.1, bf16[2048,512]{1,0:T(8,128)(2,1)} %v.1, bf16[2048,512]{1,0:T(8,128)(2,1)} %g.1, f32[2,2048]{1,0:T(2,128)} %ld.1, bf16[512,2048]{1,0:T(8,128)(2,1)} %wo.1, bf16[128,2048]{1,0:T(8,128)(2,1)} %x_ref.1, ...), custom_call_target="tpu_custom_call" | custom-call | tf_op jit(solution)/shard_map/layer/pallas_call | solution.py:692
  122.2 0.0 copy-start
  122.2 3.2 %copy.20 = bf16[512,2048]{1,0:T(8,128)(2,1)} copy(bf16[512,2048]{1,0:T(8,128)(2,1)} %get-tuple-element.4) | data formatting | bytes 4194304
  125.4 0.0 copy-done
  125.4 0.8 copy.21
Async XLA Ops:
  122.2 3.2 %copy-start = (bf16[128,2048]{1,0:T(8,128)(2,1)S(1)}, bf16[128,2048]{1,0:T(8,128)(2,1)}, u32[]{:S(2)}) copy-start(bf16[128,2048]{1,0:T(8,128)(2,1)} %get-tuple-element.5) | copy-start | bytes 1572868

commit v5 on v4

--- a/solution.py
+++ b/solution.py
@@ -52,10 +52,8 @@
     def rows(first, n):
         return pl.ds(pl.multiple_of(first, 16), n)
 
-    whole = pl.ds(0, 2048)
-    direct, half0, half1 = pl.ds(0, 1536), pl.ds(1536, 256), pl.ds(1792, 256)
-    r0 = c * 256 + y * 64 + z * 16
-    r1 = c * 256 + z * 64 + y * 16
+    whole, left, right = pl.ds(0, 2048), pl.ds(0, 1024), pl.ds(1024, 1024)
+    mine = rows(c * 256, 256)
     loads = {}
 
     def fetch():
@@ -65,20 +63,18 @@
             loads[name] = pltpu.make_async_copy(src, dst, s.in_sem.at[i])
             loads[name].start()
 
-    wx, wd = [], []
-
-    def spread_x():
-        for d in (1, 3, 2):
-            for h, (r, cols) in enumerate(((r0, half0), (r1, half1))):
-                i = (d - 1) * 2 + h
-                wx.append(
-                    start(wo_ref.at[rows(r, 16), cols], s.W.at[4 - d, rows(r, 16), cols], s.wx_s.at[i], s.wx_r.at[i], tp=d)
-                )
+    wd, wf = {}, []
 
     def spread_d():
-        for d in (1, 3, 2):
-            r = rows(c * 256, 256)
-            wd.append(start(wo_ref.at[r, direct], s.W.at[4 - d, r, direct], s.wd_s.at[d - 1], s.wd_r.at[d - 1], tp=d))
+        for d in (1, 3):
+            wd[d] = start(wo_ref.at[mine, whole], s.W.at[4 - d, mine, whole], s.wd_s.at[d // 2], s.wd_r.at[d // 2], tp=d)
+
+    def spread_f():
+        for d, cols in ((3, left), (1, right)):
+            wd[d].wait_recv()
+            wf.append(
+                start(s.W.at[4 - d, mine, cols], s.W.at[2, mine, cols], s.wf_s.at[d // 2], s.wf_r.at[d // 2], tp=d)
+            )
 
     def decays():
         for h in range(HEADS):
@@ -219,51 +215,17 @@
 
         lax.fori_loop(lo, hi, body, 0)
 
-    def near(axis, d, r, n, cols, ss, rs):
-        ref = s.W.at[1:4, rows(r, n), cols]
-        return copy(ref, ref, ss, rs, **{axis: d})
-
-    def ring(n, plan, ss, rs, out, into):
-        for d in (1, 3, 2):
-            for h, (axis, mine, theirs, cols) in enumerate(plan):
-                i = (d - 1) * 2 + h
-                cp = near(axis, d, mine, n, cols, ss.at[i], rs.at[i])
-                cp.start()
-                out.append(cp)
-                into.append(near(axis, d, theirs(d), n, cols, ss.at[i], rs.at[i]))
-
-    first, first_in, second, second_in, third = [], [], [], [], []
-
-    def spread_1():
-        for cp in wx:
+    def near(r):
+        ref = s.W.at[1:4, rows(r, 256), whole]
+        return copy(ref, ref, s.w3_s, s.w3_r, ep_2=1)
+
+    third = []
+
+    def spread_3():
+        for cp in wf:
             cp.wait_recv()
-        ring(
-            16,
-            (
-                ("ep_0", r0, lambda d: c * 256 + y * 64 + mod(z + 4 - d) * 16, half0),
-                ("ep_1", r1, lambda d: c * 256 + z * 64 + mod(y + 4 - d) * 16, half1),
-            ),
-            s.w1_s, s.w1_r, first, first_in,
-        )
-
-    def spread_2():
-        for cp in first_in:
-            cp.wait_recv()
-        ring(
-            64,
-            (
-                ("ep_1", c * 256 + y * 64, lambda d: c * 256 + mod(y + 4 - d) * 64, half0),
-                ("ep_0", c * 256 + z * 64, lambda d: c * 256 + mod(z + 4 - d) * 64, half1),
-            ),
-            s.w2_s, s.w2_r, second, second_in,
-        )
-
-    def spread_3():
-        for cp in second_in + wd:
-            cp.wait_recv()
-        cp = near("ep_2", 1, c * 256, 256, whole, s.w3_s, s.w3_r)
-        cp.start()
-        third.extend([cp, near("ep_2", 1, (1 - c) * 256, 256, whole, s.w3_s, s.w3_r)])
+        third.extend([near(c * 256), near((1 - c) * 256)])
+        third[0].start()
 
     sends = {}
 
@@ -314,7 +276,7 @@
         lax.fori_loop(lo, hi, body, 0)
 
     def finish():
-        for cp in wx + wd + first + second + third[:1] + list(sends.values()) + sum(flying.values(), []):
+        for cp in list(wd.values()) + wf + third[:1] + list(sends.values()) + sum(flying.values(), []):
             cp.wait_send()
 
     def drain():
@@ -326,8 +288,8 @@
         loads["g"].wait()
 
     return dict(
-        fetch=fetch, spread_x=spread_x, decays=decays, summary=summary, publish=publish, absorb=absorb, inside=inside,
-        spread_1=spread_1, spread_2=spread_2, spread_3=spread_3, outer=outer, ready=ready, project=project,
+        fetch=fetch, decays=decays, summary=summary, publish=publish, absorb=absorb, inside=inside,
+        spread_3=spread_3, spread_f=spread_f, outer=outer, ready=ready, project=project,
         finish=finish, gate_in=gate_in, drain=drain, swap=swap, settle=settle, spread_d=spread_d,
     )
 
@@ -362,15 +324,26 @@
         s.meta[0, 0:TOP, :] = rt_ref[...].astype(F32)
         s.meta[0, TOP : 2 * TOP, :] = wt_ref[...]
         for d in (1, 3, 2):
-            a = start(s.meta.at[0], s.meta.at[4 - d], s.gm_s.at[d - 1], s.gm_r.at[d - 1], tp=d)
-            b = start(s.X.at[0], s.X.at[4 - d], s.gx_s.at[d - 1], s.gx_r.at[d - 1], tp=d)
-            gathers[4 - d] = (a, b)
-            sends.extend([a, b])
+            sends.append(start(s.meta.at[0], s.meta.at[4 - d], s.gm_s.at[d - 1], s.gm_r.at[d - 1], tp=d))
+            gathers[4 - d] = [sends[-1]]
+        for d in (1, 3):
+            sends.append(start(s.X.at[0], s.X.at[4 - d], s.gx_s.at[d // 2], s.gx_r.at[d // 2], tp=d))
+            gathers[4 - d].append(sends[-1])
+
+    def group(ss, rs, gg, h, n):
+        ref = s.W.at[0, 0:n, :]
+        return ctx.copy(ref, ref, ss.at[gg, h], rs.at[gg, h], tp=1)
 
     def build(gg):
         if gg:
             for cp in gathers[gg]:
                 cp.wait_recv()
+            if gg != 2:
+                part = pl.ds((gg // 2) * HALF, HALF)
+                sends.append(
+                    start(s.X.at[gg, :, part], s.X.at[2, :, part], s.gf_s.at[gg // 2], s.gf_r.at[gg // 2], tp=4 - gg)
+                )
+                gathers[2].append(sends[-1])
         rt = s.meta[gg, 0:TOP, :]
         wt = s.meta[gg, TOP : 2 * TOP, :]
         ident = (iota((N_EP, N_TOK), 0) * 4 + x).astype(F32)
@@ -400,23 +373,14 @@
             s.M[gg, 1, y, zz] = s.D[gg, 1, zz, y]
         for d in (1, 3, 2):
             zp, yp = mod(z + d), mod(y + d)
-            first[gg, 0].append(
-                start(s.D.at[gg, 0, zp], s.M.at[gg, 0, z], s.a_s.at[gg, 0, d - 1], s.a_r.at[gg, 0, d - 1], ep_0=d)
-            )
-            first[gg, 1].append(
-                start(s.D.at[gg, 1, :, yp], s.M.at[gg, 1, y], s.a_s.at[gg, 1, d - 1], s.a_r.at[gg, 1, d - 1], ep_1=d)
-            )
-
-    first = {(gg, h): [] for gg in range(4) for h in range(2)}
-    second = {(gg, h): [] for gg in range(4) for h in range(2)}
-    third = {(gg, h): [] for gg in range(4) for h in range(2)}
-    fourth = {(gg, h): [] for gg in range(4) for h in range(2)}
+            start(s.D.at[gg, 0, zp], s.M.at[gg, 0, z], s.a_s.at[gg, 0], s.a_r.at[gg, 0], ep_0=d)
+            start(s.D.at[gg, 1, :, yp], s.M.at[gg, 1, y], s.a_s.at[gg, 1], s.a_r.at[gg, 1], ep_1=d)
+
     hops = [(1, 0), (3, 0), (1, 1), (3, 1), (2, 0), (2, 1), (0, 1)]
 
     def relay(gg):
         for h in range(2):
-            for cp in first[gg, h]:
-                cp.wait_recv()
+            group(s.a_s, s.a_r, gg, h, 96).wait_recv()
             for i, (d, e) in enumerate(hops):
                 zp, yp, cp_ = mod(z + d), mod(y + d), lax.rem(c + e, 2)
                 if h == 0:
@@ -425,7 +389,7 @@
                 else:
                     src, dst = s.M.at[gg, 1, :, zp, cp_], s.V.at[gg, 1, z, :, c]
                     to = {"ep_0": d, "ep_2": e}
-                second[gg, h].append(start(src, dst, s.b_s.at[gg, h, i], s.b_r.at[gg, h, i], **to))
+                start(src, dst, s.b_s.at[gg, h], s.b_r.at[gg, h], **to)
             for k in range(4):
                 if h == 0:
                     s.V[gg, 0, k, y, c] = s.M[gg, 0, k, y, c]
@@ -434,8 +398,7 @@
 
     def expert(gg):
         for h in range(2):
-            for cp in second[gg, h]:
-                cp.wait_recv()
+            group(s.b_s, s.b_r, gg, h, 112).wait_recv()
         a = s.V[gg, 0].reshape(ROWS, HALF)
         b = s.V[gg, 1].reshape(ROWS, HALF)
         gate = dot(a, s.wg[0:HALF]) + dot(b, s.wg[HALF:])
@@ -455,7 +418,7 @@
                 else:
                     src, dst = s.V.at[gg, 1, zp, :, cp_], s.N.at[gg, 1, :, z, c]
                     to = {"ep_0": d, "ep_2": e}
-                third[gg, h].append(start(src, dst, s.c_s.at[gg, h, i], s.c_r.at[gg, h, i], **to))
+                start(src, dst, s.c_s.at[gg, h], s.c_r.at[gg, h], **to)
             for k in range(4):
                 if h == 0:
                     s.N[gg, 0, k, y, c] = s.V[gg, 0, k, y, c]
@@ -464,15 +427,13 @@
 
     def relay_back(gg):
         for h in range(2):
-            for cp in third[gg, h]:
-                cp.wait_recv()
+            group(s.c_s, s.c_r, gg, h, 112).wait_recv()
             for d in (1, 3, 2):
                 zp, yp = mod(z + d), mod(y + d)
                 if h == 0:
-                    cp = start(s.N.at[gg, 0, zp], s.B.at[gg, 0, z], s.d_s.at[gg, 0, d - 1], s.d_r.at[gg, 0, d - 1], ep_0=d)
+                    start(s.N.at[gg, 0, zp], s.B.at[gg, 0, z], s.d_s.at[gg, 0], s.d_r.at[gg, 0], ep_0=d)
                 else:
-                    cp = start(s.N.at[gg, 1, yp], s.B.at[gg, 1, :, y], s.d_s.at[gg, 1, d - 1], s.d_r.at[gg, 1, d - 1], ep_1=d)
-                fourth[gg, h].append(cp)
+                    start(s.N.at[gg, 1, yp], s.B.at[gg, 1, :, y], s.d_s.at[gg, 1], s.d_r.at[gg, 1], ep_1=d)
             if h == 0:
                 s.B[gg, 0, z] = s.N[gg, 0, z]
             else:
@@ -484,8 +445,7 @@
     def fold(gg):
         for h in range(2):
             cols = slice(h * HALF, (h + 1) * HALF)
-            for cp in fourth[gg, h]:
-                cp.wait_recv()
+            group(s.d_s, s.d_r, gg, h, 96).wait_recv()
             back = s.B[gg, h].reshape(ROWS, HALF)
             part = dot(s.whi[gg], back, TN) + dot(s.wlo[gg], back, TN)
             if gg == 0:
@@ -516,10 +476,10 @@
             s.res[:, cols] = total.astype(BF16)
         out = pltpu.make_async_copy(s.res, out_ref, s.res_sem)
         out.start()
-        for group in (first, second, third, fourth):
-            for cps in group.values():
-                for cp in cps:
-                    cp.wait_send()
+        for gg in range(4):
+            for h in range(2):
+                for ss, rs, n in ((s.a_s, s.a_r, 96), (s.b_s, s.b_r, 112), (s.c_s, s.c_r, 112), (s.d_s, s.d_r, 96)):
+                    group(ss, rs, gg, h, n).wait_send()
         for cp in list(reduces.values()) + sends:
             cp.wait_send()
         out.wait()
@@ -587,9 +547,9 @@
     acc=pltpu.VMEM((N_TOK, 2048), F32),
     P=pltpu.VMEM((3, 2, N_TOK, HALF), BF16), G=pltpu.VMEM((3, 2, N_TOK, HALF), BF16),
     load=DMA((6,)),
-    gm_s=DMA((3,)), gm_r=DMA((3,)), gx_s=DMA((3,)), gx_r=DMA((3,)),
-    a_s=DMA((4, 2, 3)), a_r=DMA((4, 2, 3)), b_s=DMA((4, 2, 7)), b_r=DMA((4, 2, 7)),
-    c_s=DMA((4, 2, 7)), c_r=DMA((4, 2, 7)), d_s=DMA((4, 2, 3)), d_r=DMA((4, 2, 3)),
+    gm_s=DMA((3,)), gm_r=DMA((3,)), gx_s=DMA((2,)), gx_r=DMA((2,)), gf_s=DMA((2,)), gf_r=DMA((2,)),
+    a_s=DMA((4, 2)), a_r=DMA((4, 2)), b_s=DMA((4, 2)), b_r=DMA((4, 2)),
+    c_s=DMA((4, 2)), c_r=DMA((4, 2)), d_s=DMA((4, 2)), d_r=DMA((4, 2)),
     e_s=DMA((3, 2)), e_r=DMA((3, 2)),
     q=pltpu.VMEM((2048, 256), BF16), k=pltpu.VMEM((2048, 256), BF16),
     v=pltpu.VMEM((2048, 512), BF16), g=pltpu.VMEM((2048, 512), BF16),
@@ -604,8 +564,8 @@
     chip_S=pltpu.VMEM((DK, DV), F32), chip_f=pltpu.VMEM((1, DV), F32), got_e=pltpu.VMEM((DK, DV), F32),
     end_s=DMA, end_r=DMA,
     mix=pltpu.VMEM((512, 2048), BF16), res=pltpu.VMEM((N_TOK, 2048), BF16), out_sem=DMA((4,)), res_sem=DMA,
-    in_sem=DMA((5,)), wx_s=DMA((6,)), wx_r=DMA((6,)), wd_s=DMA((3,)), wd_r=DMA((3,)),
-    w1_s=DMA((6,)), w1_r=DMA((6,)), w2_s=DMA((6,)), w2_r=DMA((6,)), w3_s=DMA, w3_r=DMA,
+    in_sem=DMA((5,)), wd_s=DMA((2,)), wd_r=DMA((2,)), wf_s=DMA((2,)), wf_r=DMA((2,)),
+    w3_s=DMA, w3_r=DMA,
     pre_s=DMA((7,)), pre_r=DMA((7,)), ret_s=DMA((3,)), ret_r=DMA((3,)),
 )
 
@@ -622,23 +582,20 @@
     m = Names()
     a.__dict__.update(moe_steps(ctx, x_ref, gain_ref, rt_ref, wt_ref, wg, wu, wd, sg, su, sd, moe_ref, s))
     m.__dict__.update(mixer_steps(ctx, q, k, v, g, ld, wo, mix_ref, s))
-    m.spread_x()
     m.fetch()
     a.rows_out()
     a.build(0)
-    m.spread_d()
     m.decays()
-    m.spread_1()
     m.summary()
     m.publish("ep_2")
     a.shared()
-    m.spread_2()
     m.absorb("ep_2")
     m.publish("ep_1")
     a.relay(0)
     m.inside(0, 4)
     a.build(1)
     a.build(3)
+    m.spread_d()
     m.absorb("ep_1")
     m.publish("ep_0")
     m.inside(4, 8)
@@ -655,6 +612,7 @@
     m.gate_in()
     a.expert(1)
     a.relay(2)
+    m.spread_f()
     a.give_back(1)
     m.outer(1)
     m.outer(3)

time: 129 us -> 121 us (0.938)
  Pallas kernels: 122 us -> 115 us
    pallas_call x1, Pallas kernels: 122 us -> 115 us  [local(): pl.pallas_call(layer_kernel, name='layer', out_shape=(jax.ShapeDtypeStruc...]
where the time goes in v5:
time: 121 us; the launch traced here: 119 us
  Pallas kernels  115 us (95%)
  local copies, waits for them, and re-layouts  4.01 us (3%)
    pallas_call x1, Pallas kernels, local(): pl.pallas_call(layer_kernel, name='layer', out_shape=(jax.ShapeDtypeStruc...  115 us
    unnamed x4, local copies, waits for them, and re-layouts  4.01 us

profile of v5, /device:TPU:6, one launch (start us, length us, event | category | flops | bytes accessed | tf_op | source)
XLA Modules:
  0.0 119.2 jit_solution(9236459942781205746)
XLA Ops:
  0.6 114.5 %layer.1 = (bf16[512,2048]{1,0:T(8,128)(2,1)}, bf16[128,2048]{1,0:T(8,128)(2,1)}) custom-call(bf16[2048,256]{1,0:T(8,128)(2,1)} %q.1, bf16[2048,256]{1,0:T(8,128)(2,1)} %k.1, bf16[2048,512]{1,0:T(8,128)(2,1)} %v.1, bf16[2048,512]{1,0:T(8,128)(2,1)} %g.1, f32[2,2048]{1,0:T(2,128)} %ld.1, bf16[512,2048]{1,0:T(8,128)(2,1)} %wo.1, bf16[128,2048]{1,0:T(8,128)(2,1)} %x_ref.1, ...), custom_call_target="tpu_custom_call" | custom-call | tf_op jit(solution)/shard_map/layer/pallas_call | solution.py:650
  115.1 0.0 copy-start
  115.2 3.2 %copy.20 = bf16[512,2048]{1,0:T(8,128)(2,1)} copy(bf16[512,2048]{1,0:T(8,128)(2,1)} %get-tuple-element.4) | data formatting | bytes 4194304
  118.4 0.0 copy-done
  118.4 0.8 copy.21
Async XLA Ops:
  115.1 3.2 %copy-start = (bf16[128,2048]{1,0:T(8,128)(2,1)S(1)}, bf16[128,2048]{1,0:T(8,128)(2,1)}, u32[]{:S(2)}) copy-start(bf16[128,2048]{1,0:T(8,128)(2,1)} %get-tuple-element.5) | copy-start | bytes 1572868
